TPU v7x, 32 devices: a whole 2x2x4 slice. The times are simulated.
32 devices in a mesh: sp: 8 (over z, x), tp: 4 (over y, core).
Axes of the slice: x: 2, y: 2, z: 4, core: 2. Of those that a mesh axis runs over, the one named last changes fastest.
Arguments:
- tokens: bfloat16 [2, 1536, 4096], P(None, 'sp', 'tp'), may hold values from -12 to 12
- query_weight: bfloat16 [4096, 2048], P(None, 'tp'), may hold values from -0.09375 to 0.09375
- key_weight: bfloat16 [4096, 2048], P(None, 'tp'), may hold values from -0.09375 to 0.09375
- value_weight: bfloat16 [4096, 2048], P(None, 'tp'), may hold values from -0.09375 to 0.09375
- gate_weight: bfloat16 [4096, 2048], P(None, 'tp'), may hold values from -0.09375 to 0.09375
- beta_weight: bfloat16 [4096, 16], P(None, 'tp'), may hold values from -0.09375 to 0.09375
- decay_weight: bfloat16 [4096, 16], P(None, 'tp'), may hold values from -0.09375 to 0.09375
- beta_bias: float32 [16], P('tp'), may hold values from -6 to -3
- rate_log: float32 [16], P('tp'), may hold values from -12 to -2.5
- out_gain: float32 [128], replicated, may hold values from 0.1 to 1.9
- new_query: bfloat16 [2, 16, 128], P(None, 'tp'), may hold values from -6 to 6
- new_key: bfloat16 [2, 16, 128], P(None, 'tp'), may hold values from -6 to 6
- new_value: bfloat16 [2, 16, 128], P(None, 'tp'), may hold values from -6 to 6
- new_beta: float32 [2, 16], P(None, 'tp'), may hold values from 0.1 to 0.9
- new_decay: float32 [2, 16], P(None, 'tp'), may hold values from 0.3 to 1
Outputs:
- mixed_out: bfloat16 [2, 1536, 2048], P(None, 'sp', 'tp')
- cache: bfloat16 [2, 16, 128, 128], P(None, 'tp', 'sp')
- first_out: float32 [2, 2048], P(None, 'tp')
All inputs are finite; a program needn't handle non-finite values.
Results may differ from a plain program's by a relative error of at most 0.0073.
Values may be sent and summed in bfloat16 or wider, within the bound.
A program may use at most 64 MiB of HBM per device.

v0:
```python
import functools

import jax
import jax.numpy as jnp
from jax import lax
from jax.experimental import pallas as pl
from jax.experimental.pallas import tpu as pltpu
from jax.sharding import PartitionSpec as P

unit_floor = 1.0
norm_floor = 0.001
highest = lax.Precision.HIGHEST
MESH = pl.DeviceIdType.MESH
PAD = 8
f32 = jnp.float32
bf16 = jnp.bfloat16

NN = (((1,), (0,)), ((), ()))
NT = (((1,), (1,)), ((), ()))
TN = (((0,), (0,)), ((), ()))


def dot(left, right, dims=NN, precision=None):
    return lax.dot_general(left, right, dims, precision=precision, preferred_element_type=f32)


def gather_kernel(
    n, seqs, x_ref, wq_ref, wk_ref, wv_ref, wg_ref, bw_ref, dw_ref, out_ref,
    small_ref, bd_ref, xs, wbuf, acc, sacc, wsem, cross_sem, part_sem, fwd_sem, rx,
):
    me = lax.axis_index("tp")
    y, c = me // 2, lax.rem(me, 2)
    chips = n // 2
    rows, kd = x_ref.shape
    span = rows // seqs
    _, chunks, _, kc = xs.shape
    partner = y * 2 + (1 - c)
    weights = (wq_ref, wk_ref, wv_ref, wg_ref)

    barrier = pltpu.get_barrier_semaphore()
    pl.semaphore_signal(barrier, inc=1, device_id={"tp": partner}, device_id_type=MESH)
    for d in range(1, chips):
        to = lax.rem(y + d, chips) * 2 + c
        pl.semaphore_signal(barrier, inc=1, device_id={"tp": to}, device_id_type=MESH)

    order = [me, partner]
    for d in range(1, chips):
        source = lax.rem(y - d + chips, chips)
        order += [source * 2 + c, source * 2 + (1 - c)]

    def weight_copy(w, slot):
        start = pl.multiple_of(order[slot] * kd, kd)
        return pltpu.make_async_copy(
            weights[w].at[pl.ds(start, kd), :], wbuf.at[w, slot], wsem.at[w, slot]
        )

    for slot in range(n):
        for w in range(4):
            weight_copy(w, slot).start()
    bd_ref[...] = jnp.zeros_like(bd_ref)
    bd_ref[0 : bw_ref.shape[0]] = bw_ref[...]
    bd_ref[PAD : PAD + dw_ref.shape[0]] = dw_ref[...]
    pl.semaphore_wait(barrier, chips)

    def cols(ck):
        return pl.ds(ck * kc, kc)

    def cross_copy(d, ck):
        to = lax.rem(y + d, chips) * 2 + c
        return pltpu.make_async_remote_copy(
            src_ref=x_ref.at[:, cols(ck)], dst_ref=xs.at[me, ck],
            send_sem=cross_sem.at[d - 1, ck], recv_sem=rx.at[me, ck],
            device_id={"tp": to}, device_id_type=MESH,
        )

    def part_copy(ck):
        return pltpu.make_async_remote_copy(
            src_ref=x_ref.at[:, cols(ck)], dst_ref=xs.at[me, ck],
            send_sem=part_sem.at[ck], recv_sem=rx.at[me, ck],
            device_id={"tp": partner}, device_id_type=MESH,
        )

    def fwd_copy(d, ck):
        b = order[2 * d]
        return pltpu.make_async_remote_copy(
            src_ref=xs.at[b, ck], dst_ref=xs.at[b, ck],
            send_sem=fwd_sem.at[d - 1, ck], recv_sem=rx.at[b, ck],
            device_id={"tp": partner}, device_id_type=MESH,
        )

    def arrive(b, ck):
        pltpu.make_async_remote_copy(
            src_ref=xs.at[b, ck], dst_ref=xs.at[b, ck],
            send_sem=part_sem.at[ck], recv_sem=rx.at[b, ck],
            device_id={"tp": partner}, device_id_type=MESH,
        ).wait_recv()

    for ck in range(chunks):
        for d in range(1, chips):
            cross_copy(d, ck).start()
    for ck in range(chunks):
        part_copy(ck).start()

    def small(x, start, depth, first):
        piece = bd_ref[:, pl.ds(pl.multiple_of(start, depth), depth)]
        for s in range(seqs):
            term = dot(piece, x[s * span : (s + 1) * span], NT)
            sacc[s] = term if first else sacc[s] + term

    for w in range(4):
        weight_copy(w, 0).wait()
        acc[w] = dot(x_ref[...], wbuf[w, 0])
    small(x_ref[...], me * kd, kd, True)

    def use(slot, ck):
        b = order[slot]
        x = xs[b, ck]
        for w in range(4):
            if ck == 0:
                weight_copy(w, slot).wait()
            acc[w] += dot(x, wbuf[w, slot, pl.ds(ck * kc, kc), :])
        small(x, b * kd + ck * kc, kc, False)

    for ck in range(chunks):
        arrive(partner, ck)
        use(1, ck)
    for d in range(1, chips):
        for ck in range(chunks):
            arrive(order[2 * d], ck)
            fwd_copy(d, ck).start()
            use(2 * d, ck)
            arrive(order[2 * d + 1], ck)
            use(2 * d + 1, ck)
    for w in range(4):
        out_ref[w] = acc[w].astype(bf16)
    small_ref[...] = sacc[...]
    for ck in range(chunks):
        part_copy(ck).wait_send()
        for d in range(1, chips):
            cross_copy(d, ck).wait_send()
            fwd_copy(d, ck).wait_send()


def gather_project(n, seqs, tokens, weights, bw, dw):
    rows, kd = tokens.shape
    width = weights[0].shape[1]
    kc = 256 if kd % 256 == 0 else kd
    chunks = kd // kc
    chips = n // 2
    span = rows // seqs
    return pl.pallas_call(
        functools.partial(gather_kernel, n, seqs),
        out_shape=(
            jax.ShapeDtypeStruct((4, rows, width), bf16),
            jax.ShapeDtypeStruct((seqs, 2 * PAD, span), f32),
        ),
        in_specs=[pl.BlockSpec(memory_space=pltpu.VMEM)]
        + [pl.BlockSpec(memory_space=pl.ANY)] * 4
        + [pl.BlockSpec(memory_space=pltpu.VMEM)] * 2,
        out_specs=(pl.BlockSpec(memory_space=pltpu.VMEM),) * 2,
        scratch_shapes=[
            pltpu.VMEM((2 * PAD, bw.shape[1]), bf16),
            pltpu.VMEM((n, chunks, rows, kc), bf16),
            pltpu.VMEM((4, n, kd, width), bf16),
            pltpu.VMEM((4, rows, width), f32),
            pltpu.VMEM((seqs, 2 * PAD, span), f32),
            pltpu.SemaphoreType.DMA((4, n)),
            pltpu.SemaphoreType.DMA((chips - 1, chunks)),
            pltpu.SemaphoreType.DMA((chunks,)),
            pltpu.SemaphoreType.DMA((chips - 1, chunks)),
            pltpu.SemaphoreType.DMA((n, chunks)),
        ],
        compiler_params=pltpu.CompilerParams(
            collective_id=0, has_side_effects=True, vmem_limit_bytes=60 * 1024 * 1024
        ),
    )(tokens, *weights, bw, dw)


def unit_rows(values):
    return values * lax.rsqrt(jnp.sum(values * values, axis=-1, keepdims=True) + unit_floor)


def delta_kernel(
    n, seqs, heads, group, rows_ref, small_ref, bias_ref, rate_ref, gain_ref, nq_ref, nk_ref, nv_ref,
    nb_ref, nd_ref, mixed_ref, cache_ref, first_ref,
    cum_row, cum_col, beta_col, local_out, reach, out_box, in_box, back_out, back_in, tail_out,
    tail_in, send1, recv1, send2, recv2, send3, recv3,
):
    me = lax.axis_index("sp")
    pairs = seqs * heads
    span = rows_ref.shape[1] // seqs
    extent = rows_ref.shape[2] // heads
    key_rows = extent // n

    barrier = pltpu.get_barrier_semaphore()
    for d in range(1, n):
        to = lax.rem(me + d, n)
        pl.semaphore_signal(barrier, inc=1, device_id={"sp": to}, device_id_type=MESH)

    row = lax.broadcasted_iota(jnp.int32, (span, span), 0)
    col = lax.broadcasted_iota(jnp.int32, (span, span), 1)
    upper = jnp.where(row <= col, 1.0, 0.0)
    slot_of = lax.broadcasted_iota(jnp.int32, (PAD, 1), 0)
    bias = jnp.zeros((PAD, 1), f32)
    rate = jnp.zeros((PAD, 1), f32)
    for h in range(heads):
        bias = jnp.where(slot_of == h, bias_ref[h], bias)
        rate = jnp.where(slot_of == h, rate_ref[h], rate)
    for s in range(seqs):
        beta = jax.nn.sigmoid(small_ref[s, 0:PAD, :] + bias)
        pre = small_ref[s, PAD : 2 * PAD, :]
        soft = jnp.maximum(pre, 0.0) + jnp.log1p(jnp.exp(-jnp.abs(pre)))
        cum = dot(-jnp.exp(rate) * soft, upper, NN, highest)
        cum_row[s] = cum
        cum_col[s] = cum.T
        beta_col[s] = beta.T
    eye_lane = lax.broadcasted_iota(jnp.int32, (extent, extent), 0) == lax.broadcasted_iota(
        jnp.int32, (extent, extent), 1
    )
    pl.semaphore_wait(barrier, n - 1)

    def send_box(p):
        return pltpu.make_async_remote_copy(
            src_ref=out_box.at[p], dst_ref=in_box.at[me],
            send_sem=send1.at[p], recv_sem=recv1.at[me],
            device_id={"sp": p}, device_id_type=MESH,
        )

    def local_group(i, _):
        ps = [lax.rem(me + 1 + i * group + j, pairs) for j in range(group)]
        each = []
        for p in ps:
            s, h = p // heads, lax.rem(p, heads)
            at = pl.ds(pl.multiple_of(s * span, span), span)
            lanes = pl.ds(pl.multiple_of(h * extent, extent), extent)
            q = unit_rows(rows_ref[0, at, lanes].astype(f32))
            k = unit_rows(rows_ref[1, at, lanes].astype(f32))
            v = rows_ref[2, at, lanes].astype(f32)
            pick = lax.broadcasted_iota(jnp.int32, (span, PAD), 1) == h
            cumc = jnp.sum(jnp.where(pick, cum_col[s], 0.0), axis=1, keepdims=True)
            beta = jnp.sum(jnp.where(pick, beta_col[s], 0.0), axis=1, keepdims=True)
            cumr = cum_row[s, pl.ds(h, 1), :]
            causal = row >= col
            weights = jnp.where(causal, jnp.exp(jnp.where(causal, cumc - cumr, 0.0)), 0.0)
            kb = k * beta
            kh = k.astype(bf16)
            lower = jnp.where(row > col, dot(kb.astype(bf16), kh, NT) * weights, 0.0)
            score = (dot(q.astype(bf16), kh, NT) * weights).astype(bf16)
            grow = jnp.exp(cumc)
            right = jnp.concatenate([v * beta, kb * grow], axis=1).astype(bf16)
            last = cumc[span - 1 :, :]
            kdec = (k * jnp.exp(last - cumc)).astype(bf16)
            each.append([lower, score, right, kdec, q * grow, jnp.exp(last)])
        unit = jnp.where(row == col, 1.0, 0.0)
        pair_mask = ((row >> 1) == (col >> 1)) & (row > col)
        inv = [unit - jnp.where(pair_mask, e[0], 0.0) for e in each]
        level = 1
        while (1 << level) < span:
            mask = ((row >> (level + 1)) == (col >> (level + 1))) & ((row >> level) > (col >> level))
            inv_h = [m.astype(bf16) for m in inv]
            mid = [
                dot(jnp.where(mask, e[0], 0.0).astype(bf16), m).astype(bf16)
                for e, m in zip(each, inv_h)
            ]
            inv = [m - dot(mh, t) for m, mh, t in zip(inv, inv_h, mid)]
            level += 1
        uw = [dot(m.astype(bf16), e[2]).astype(bf16) for m, e in zip(inv, each)]
        out = [dot(e[1], u) for e, u in zip(each, uw)]
        fin = [dot(e[3], u, TN) for e, u in zip(each, uw)]
        for p, e, o, z in zip(ps, each, out, fin):
            local_out[p] = o[:, :extent]
            reach[p] = (e[4] - o[:, extent:]).astype(bf16)
            step = (jnp.where(eye_lane, e[5] - 1.0, 0.0) - z[:, extent:]).astype(bf16)
            state = z[:, :extent].astype(bf16)

            @pl.when(p == me)
            def _():
                in_box[me, 0] = step
                in_box[me, 1] = state

            @pl.when(p != me)
            def _():
                out_box[p, 0] = step
                out_box[p, 1] = state
                send_box(p).start()

        return 0

    lax.fori_loop(0, pairs // group, local_group, 0)

    def back_copy(j):
        return pltpu.make_async_remote_copy(
            src_ref=back_out.at[j], dst_ref=back_in.at[me],
            send_sem=send2.at[j], recv_sem=recv2.at[me],
            device_id={"sp": j}, device_id_type=MESH,
        )

    def tail_copy(j):
        return pltpu.make_async_remote_copy(
            src_ref=tail_out.at[j], dst_ref=tail_in.at[me],
            send_sem=send3.at[j], recv_sem=recv3.at[me],
            device_id={"sp": j}, device_id_type=MESH,
        )

    @pl.when(me < pairs)
    def _():
        def chain(j, state):
            half = state.astype(bf16)

            @pl.when(j == me)
            def _():
                back_in[me] = half

            @pl.when(j != me)
            def _():
                back_out[j] = half
                back_copy(j).start()
                pltpu.make_async_remote_copy(
                    src_ref=out_box.at[0], dst_ref=in_box.at[j],
                    send_sem=send1.at[0], recv_sem=recv1.at[j],
                    device_id={"sp": j}, device_id_type=MESH,
                ).wait_recv()

            return state + dot(in_box[j, 0], half) + in_box[j, 1].astype(f32)

        final = lax.fori_loop(0, n, chain, jnp.zeros((extent, extent), f32))
        memory = final.astype(bf16).astype(f32)
        shape3 = nq_ref.shape
        mine = (
            lax.broadcasted_iota(jnp.int32, shape3, 0) * heads
            + lax.broadcasted_iota(jnp.int32, shape3, 1)
        ) == me

        def own(ref):
            kept = jnp.where(mine, ref[...].astype(f32), 0.0)
            return jnp.sum(jnp.sum(kept, axis=0), axis=0, keepdims=True)

        qn, kn = unit_rows(own(nq_ref)), unit_rows(own(nk_ref))
        both = jnp.concatenate([jnp.broadcast_to(qn, (PAD, extent)), jnp.broadcast_to(kn, (PAD, extent))], axis=0)
        reads = dot(both, memory, NN, highest)
        recall, retrieve = reads[0:1], reads[PAD : PAD + 1]
        s, h = me // heads, lax.rem(me, heads)
        beta_new, decay_new = nb_ref[s, h], nd_ref[s, h]
        fresh = own(nv_ref) - decay_new * retrieve
        meet = jnp.sum(kn * qn, axis=-1, keepdims=True)
        read = decay_new * recall + (beta_new * meet) * fresh
        norm = lax.rsqrt(jnp.mean(read * read, axis=-1, keepdims=True) + norm_floor)
        answer = jnp.broadcast_to(read * norm * gain_ref[...], (PAD, extent))
        for j in range(n):
            tail_out[j, 0:key_rows, :] = memory[j * key_rows : (j + 1) * key_rows]
            tail_out[j, tail_out.shape[1] - PAD :, :] = answer

        def push(j, _):
            @pl.when(j == me)
            def _():
                tail_in[me] = tail_out[me]

            @pl.when(j != me)
            def _():
                tail_copy(j).start()

            return 0

        lax.fori_loop(0, n, push, 0)

    gain = gain_ref[...]

    def finish(i, _):
        p = lax.rem(me + i, pairs)
        s, h = p // heads, lax.rem(p, heads)
        at = pl.ds(pl.multiple_of(s * span, span), span)
        lanes = pl.ds(pl.multiple_of(h * extent, extent), extent)

        @pl.when(p != me)
        def _():
            pltpu.make_async_remote_copy(
                src_ref=back_out.at[0], dst_ref=back_in.at[p],
                send_sem=send2.at[0], recv_sem=recv2.at[p],
                device_id={"sp": p}, device_id_type=MESH,
            ).wait_recv()

        o = local_out[p] + dot(reach[p], back_in[p])
        norm = lax.rsqrt(jnp.mean(o * o, axis=-1, keepdims=True) + norm_floor)
        gate = rows_ref[3, at, lanes].astype(f32)
        mixed_ref[at, lanes] = (o * norm * gain * (gate * jax.nn.sigmoid(gate))).astype(bf16)
        return 0

    lax.fori_loop(0, pairs, finish, 0)

    for p in range(pairs):

        @pl.when(p != me)
        def _():
            pltpu.make_async_remote_copy(
                src_ref=tail_out.at[0], dst_ref=tail_in.at[p],
                send_sem=send3.at[0], recv_sem=recv3.at[p],
                device_id={"sp": p}, device_id_type=MESH,
            ).wait_recv()

        cache_ref[p] = tail_in[p, 0:key_rows, :].astype(bf16)
        last = tail_in.shape[1]
        first_ref[p : p + 1, :] = tail_in[p, last - PAD : last - PAD + 1, :]

    for p in range(pairs):

        @pl.when(p != me)
        def _():
            send_box(p).wait_send()

    @pl.when(me < pairs)
    def _():
        for j in range(n):

            @pl.when(j != me)
            def _():
                back_copy(j).wait_send()
                tail_copy(j).wait_send()


def delta(n, seqs, heads, rows4, small, bias, rate, gain, nq, nk, nv, nb, nd):
    _, rows, width = rows4.shape
    span, extent = rows // seqs, width // heads
    pairs = seqs * heads
    key_rows = extent // n
    tail = -(-key_rows // PAD) * PAD + PAD
    vmem = pl.BlockSpec(memory_space=pltpu.VMEM)
    smem = pl.BlockSpec(memory_space=pltpu.SMEM)
    return pl.pallas_call(
        functools.partial(delta_kernel, n, seqs, heads, 2),
        out_shape=(
            jax.ShapeDtypeStruct((rows, width), bf16),
            jax.ShapeDtypeStruct((pairs, key_rows, extent), bf16),
            jax.ShapeDtypeStruct((pairs, extent), f32),
        ),
        in_specs=[vmem] * 2 + [smem] * 2 + [vmem] * 4 + [smem] * 2,
        out_specs=(vmem,) * 3,
        scratch_shapes=[
            pltpu.VMEM((seqs, PAD, span), f32),
            pltpu.VMEM((seqs, span, PAD), f32),
            pltpu.VMEM((seqs, span, PAD), f32),
            pltpu.VMEM((pairs, span, extent), f32),
            pltpu.VMEM((pairs, span, extent), bf16),
            pltpu.VMEM((pairs, 2, extent, extent), bf16),
            pltpu.VMEM((n, 2, extent, extent), bf16),
            pltpu.VMEM((n, extent, extent), bf16),
            pltpu.VMEM((pairs, extent, extent), bf16),
            pltpu.VMEM((n, tail, extent), f32),
            pltpu.VMEM((pairs, tail, extent), f32),
            pltpu.SemaphoreType.DMA((pairs,)),
            pltpu.SemaphoreType.DMA((n,)),
            pltpu.SemaphoreType.DMA((n,)),
            pltpu.SemaphoreType.DMA((pairs,)),
            pltpu.SemaphoreType.DMA((n,)),
            pltpu.SemaphoreType.DMA((pairs,)),
        ],
        compiler_params=pltpu.CompilerParams(
            collective_id=1, has_side_effects=True, vmem_limit_bytes=48 * 1024 * 1024
        ),
    )(rows4, small, bias, rate, gain, nq, nk, nv, nb, nd)


def shards(
    tokens, query_weight, key_weight, value_weight, gate_weight, beta_weight, decay_weight,
    beta_bias, rate_log, out_gain, new_query, new_key, new_value, new_beta, new_decay,
):
    seqs, span, kd = tokens.shape
    heads = rate_log.shape[0]
    extent = out_gain.shape[0]
    tp, sp = lax.axis_size("tp"), lax.axis_size("sp")
    weights = (query_weight, key_weight, value_weight, gate_weight)
    rows4, small = gather_project(tp, seqs, tokens.reshape(seqs * span, kd), weights, beta_weight.T, decay_weight.T)
    mixed, cache, first = delta(
        sp, seqs, heads, rows4, small, beta_bias, rate_log, out_gain[None], new_query, new_key, new_value,
        new_beta, new_decay,
    )
    return (
        mixed.reshape(seqs, span, heads * extent),
        cache.reshape(seqs, heads, extent // sp, extent),
        first.reshape(seqs, heads * extent),
    )


def solution(mesh):
    placed = (
        P(None, "sp", "tp"),
        P(None, "tp"),
        P(None, "tp"),
        P(None, "tp"),
        P(None, "tp"),
        P(None, "tp"),
        P(None, "tp"),
        P("tp"),
        P("tp"),
        P(),
        P(None, "tp", None),
        P(None, "tp", None),
        P(None, "tp", None),
        P(None, "tp"),
        P(None, "tp"),
    )
    return jax.shard_map(
        shards,
        mesh=mesh,
        in_specs=placed,
        out_specs=(P(None, "sp", "tp"), P(None, "tp", "sp", None), P(None, "tp")),
        check_vma=False,
    )
```

profile of v0, /device:TPU:0, one launch (start us, length us, event | category | flops | bytes accessed | tf_op | source)
XLA Modules:
  0.0 61.7 jit_solution(6960686819547109848)
XLA Ops:
  0.6 0.0 copy-start.2
  0.6 0.0 copy-start.3
  0.7 0.0 copy-start.4
  0.7 0.0 copy-start.5
  0.7 0.0 copy-start.6
  0.7 0.0 copy-start.7
  0.7 0.0 copy-start.8
  0.7 0.0 copy-start.9
  0.7 25.8 %shard_map.166 = (bf16[4,384,512]{2,1,0:T(8,128)(2,1)}, f32[2,16,192]{2,1,0:T(8,128)}) custom-call(bf16[384,1024]{1,0:T(8,128)(2,1)} %bitcast.9, bf16[4096,512]{1,0:T(8,128)(2,1)} %wq_ref.1, bf16[4096,512]{1,0:T(8,128)(2,1)} %wk_ref.1, bf16[4096,512]{1,0:T(8,128)(2,1)} %wv_ref.1, bf16[4096,512]{1,0:T(8,128)(2,1)} %wg_ref.1, bf16[4,4096]{1,0:T(4,128)(2,1)} %bitcast.10, ...), custom_call_target="tpu_custom_call" | custom-call | tf_op jit(solution)/shard_map/pallas_call | solution.py:151
  26.5 0.0 copy-done.2
  26.5 0.0 copy-done.3
  26.6 0.0 copy-done.4
  26.6 0.0 copy-done.5
  26.6 0.0 copy-done.6
  26.6 0.0 copy-done.7
  26.6 0.0 copy-done.8
  26.6 0.0 copy-done.9
  26.6 0.0 copy-start
  26.6 1.4 %copy-done = bf16[4,384,512]{2,1,0:T(8,128)(2,1)S(1)} copy-done((bf16[4,384,512]{2,1,0:T(8,128)(2,1)S(1)}, bf16[4,384,512]{2,1,0:T(8,128)(2,1)}, u32[]{:S(2)}) %copy-start) | copy-done | bytes 1572888
  28.0 0.0 copy-start.1
  28.0 0.8 %copy-done.1 = f32[2,16,192]{2,1,0:T(8,128)S(1)} copy-done((f32[2,16,192]{2,1,0:T(8,128)S(1)}, f32[2,16,192]{2,1,0:T(8,128)}, u32[]{:S(2)}) %copy-start.1) | copy-done | bytes 24600
  28.8 31.0 %shard_map.167 = (bf16[384,512]{1,0:T(8,128)(2,1)S(1)}, bf16[8,16,128]{2,1,0:T(8,128)(2,1)S(1)}, f32[8,128]{1,0:T(8,128)S(1)}) custom-call(bf16[4,384,512]{2,1,0:T(8,128)(2,1)S(1)} %copy-done, f32[2,16,192]{2,1,0:T(8,128)S(1)} %copy-done.1, f32[4]{0:T(128)S(1)} %copy-done.7, f32[4]{0:T(128)S(1)} %copy-done.8, f32[1,128]{1,0:T(1,128)S(1)} %bitcast.8, ...), custom_call_target="tpu_custom_call" | custom-call | tf_op jit(solution)/shard_map/pallas_call | solution.py:428
  59.8 0.6 reshape.21
  60.4 0.7 %copy.20 = bf16[2,192,512]{2,1,0:T(8,128)(2,1)} copy(bf16[2,192,512]{2,1,0:T(8,128)(2,1)S(1)} %bitcast.6) | data formatting | bytes 786432
  61.1 0.6 copy.21
Async XLA Ops:
  0.6 25.9 %copy-start.2 = (bf16[2,4,128]{2,1,0:T(4,128)(2,1)S(1)}, bf16[2,4,128]{2,1,0:T(4,128)(2,1)}, u32[]{:S(2)}) copy-start(bf16[2,4,128]{2,1,0:T(4,128)(2,1)} %nq_ref.1) | copy-start | bytes 6148
  0.6 25.9 %copy-start.3 = (bf16[2,4,128]{2,1,0:T(4,128)(2,1)S(1)}, bf16[2,4,128]{2,1,0:T(4,128)(2,1)}, u32[]{:S(2)}) copy-start(bf16[2,4,128]{2,1,0:T(4,128)(2,1)} %nk_ref.1) | copy-start | bytes 6148
  0.7 25.9 %copy-start.4 = (bf16[2,4,128]{2,1,0:T(4,128)(2,1)S(1)}, bf16[2,4,128]{2,1,0:T(4,128)(2,1)}, u32[]{:S(2)}) copy-start(bf16[2,4,128]{2,1,0:T(4,128)(2,1)} %nv_ref.1) | copy-start | bytes 6148
  0.7 25.9 %copy-start.5 = (f32[2,4]{1,0:T(2,128)S(1)}, f32[2,4]{1,0:T(2,128)}, u32[]{:S(2)}) copy-start(f32[2,4]{1,0:T(2,128)} %nb_ref.1) | copy-start | bytes 100
  0.7 25.9 %copy-start.6 = (f32[2,4]{1,0:T(2,128)S(1)}, f32[2,4]{1,0:T(2,128)}, u32[]{:S(2)}) copy-start(f32[2,4]{1,0:T(2,128)} %nd_ref.1) | copy-start | bytes 100
  0.7 25.9 %copy-start.7 = (f32[4]{0:T(128)S(1)}, f32[4]{0:T(128)}, u32[]{:S(2)}) copy-start(f32[4]{0:T(128)} %bias_ref.1) | copy-start | bytes 52
  0.7 25.9 %copy-start.8 = (f32[4]{0:T(128)S(1)}, f32[4]{0:T(128)}, u32[]{:S(2)}) copy-start(f32[4]{0:T(128)} %rate_ref.1) | copy-start | bytes 52
  0.7 25.9 %copy-start.9 = (f32[128]{0:T(128)S(1)}, f32[128]{0:T(128)}, u32[]{:S(2)}) copy-start(f32[128]{0:T(128)} %param.24) | copy-start | bytes 1540
  26.6 1.4 %copy-start = (bf16[4,384,512]{2,1,0:T(8,128)(2,1)S(1)}, bf16[4,384,512]{2,1,0:T(8,128)(2,1)}, u32[]{:S(2)}) copy-start(bf16[4,384,512]{2,1,0:T(8,128)(2,1)} %get-tuple-element.8.rows_ref) | copy-start | bytes 4718596
  28.0 0.8 %copy-start.1 = (f32[2,16,192]{2,1,0:T(8,128)S(1)}, f32[2,16,192]{2,1,0:T(8,128)}, u32[]{:S(2)}) copy-start(f32[2,16,192]{2,1,0:T(8,128)} %get-tuple-element.9.small_ref) | copy-start | bytes 73732
where the time goes:
time: 62.3 us; the launch traced here: 61.7 us
  Pallas kernels  56.8 us (91%)
  local copies, waits for them, and re-layouts  4.15 us (7%)
  between operations  0.79 us (1%)
    pallas_call x1, Pallas kernels, delta(): pl.pallas_call(functools.partial(delta_kernel, n, seqs, heads, 2), out_sh...  31 us
    pallas_call x1, Pallas kernels, gather_project(): pl.pallas_call(functools.partial(gather_kernel, n, seqs), out_shape=(jax....  25.8 us
    unnamed x22, local copies, waits for them, and re-layouts  3.55 us

commit v1 on v0

v1 whole, which is shorter than its diff:
```python
import functools

import jax
import jax.numpy as jnp
from jax import lax
from jax.experimental import pallas as pl
from jax.experimental.pallas import tpu as pltpu
from jax.sharding import PartitionSpec as P

unit_floor = 1.0
norm_floor = 0.001
highest = lax.Precision.HIGHEST
MESH = pl.DeviceIdType.MESH
PAD = 8
INNER, OUTER = 8, 64
f32 = jnp.float32
bf16 = jnp.bfloat16

NN = (((1,), (0,)), ((), ()))
NT = (((1,), (1,)), ((), ()))
TN = (((0,), (0,)), ((), ()))


def dot(left, right, dims=NN, precision=None):
    return lax.dot_general(left, right, dims, precision=precision, preferred_element_type=f32)


def unit_rows(values):
    return values * lax.rsqrt(jnp.sum(values * values, axis=-1, keepdims=True) + unit_floor)


def group_of(n, heads):
    g = 1
    while g < n and (g < heads or g * g < n):
        g *= 2
    return g


def fused_kernel(
    tn, sn, seqs, heads, x_ref, wq_ref, wk_ref, wv_ref, wg_ref, bw_ref, dw_ref, bias_ref, rate_ref, gain_ref,
    nq_ref, nk_ref, nv_ref, nb_ref, nd_ref, mixed_ref, cache_ref, first_ref,
    bd, xs, wbuf, acc, sacc, masks, cum_col, kh_buf, spread, uw_buf, local_out, reach, gated,
    out_box, in_box, mid_out, mid_in, back_out, back_in, tail_out, tail_in,
    xsem, wsem, cross_sem, part_sem, fwd_sem, rx, prx,
    send1, recv1, send2, recv2, send3, recv3, send4, recv4,
):
    _, _, span, kd = xs.shape
    width = wq_ref.shape[1]
    extent = width // heads
    key_rows = extent // sn
    chunks = xsem.shape[1]
    kc = kd // chunks
    tme, me = lax.axis_index("tp"), lax.axis_index("sp")
    y, c = tme // 2, lax.rem(tme, 2)
    chips = tn // 2
    partner = y * 2 + (1 - c)
    g = group_of(sn, heads)
    groups = sn // g
    team, m = me // g, lax.rem(me, g)
    weights = (wq_ref, wk_ref, wv_ref, wg_ref)

    barrier = pltpu.get_barrier_semaphore()
    pl.semaphore_signal(barrier, inc=1, device_id={"tp": partner}, device_id_type=MESH)
    for d in range(1, chips):
        to = lax.rem(y + d, chips) * 2 + c
        pl.semaphore_signal(barrier, inc=1, device_id={"tp": to}, device_id_type=MESH)
    for d in range(1, sn):
        pl.semaphore_signal(barrier, inc=1, device_id={"sp": lax.rem(me + d, sn)}, device_id_type=MESH)

    order = [tme, partner]
    for d in range(1, chips):
        source = lax.rem(y - d + chips, chips)
        order += [source * 2 + c, source * 2 + (1 - c)]

    def cols(ck):
        return pl.ds(ck * kc, kc)

    def token_copy(s, ck):
        return pltpu.make_async_copy(
            x_ref.at[pl.ds(s * span, span), cols(ck)], xs.at[tme, s, :, cols(ck)], xsem.at[s, ck]
        )

    def weight_copy(w, slot):
        start = pl.multiple_of(order[slot] * kd, kd)
        return pltpu.make_async_copy(
            weights[w].at[pl.ds(start, kd), :], wbuf.at[w, slot], wsem.at[w, slot]
        )

    for s in range(seqs):
        for ck in range(chunks):
            token_copy(s, ck).start()
    for slot in range(tn):
        for w in range(4):
            weight_copy(w, slot).start()

    bd[...] = jnp.zeros_like(bd)
    bd[0 : bw_ref.shape[0]] = bw_ref[...]
    bd[PAD : PAD + dw_ref.shape[0]] = dw_ref[...]
    row = lax.broadcasted_iota(jnp.int32, (span, span), 0)
    col = lax.broadcasted_iota(jnp.int32, (span, span), 1)
    same_in = row // INNER == col // INNER
    same_out = row // OUTER == col // OUTER
    masks[0] = jnp.where(same_in, 1.0, 0.0).astype(bf16)
    masks[1] = jnp.where(same_out & ~same_in, 1.0, 0.0).astype(bf16)
    masks[2] = jnp.where(same_out, 0.0, 1.0).astype(bf16)
    slot_of = lax.broadcasted_iota(jnp.int32, (PAD, 1), 0)
    bias = jnp.zeros((PAD, 1), f32)
    rate = jnp.zeros((PAD, 1), f32)
    for h in range(heads):
        bias = jnp.where(slot_of == h, bias_ref[h], bias)
        rate = jnp.where(slot_of == h, rate_ref[h], rate)
    pl.semaphore_wait(barrier, chips + sn - 1)

    def cross_copy(d, s, ck):
        to = lax.rem(y + d, chips) * 2 + c
        return pltpu.make_async_remote_copy(
            src_ref=xs.at[tme, s, :, cols(ck)], dst_ref=xs.at[tme, s, :, cols(ck)],
            send_sem=cross_sem.at[d - 1, s, ck], recv_sem=rx.at[tme, s, ck],
            device_id={"tp": to}, device_id_type=MESH,
        )

    def part_copy(s):
        return pltpu.make_async_remote_copy(
            src_ref=xs.at[tme, s], dst_ref=xs.at[tme, s],
            send_sem=part_sem.at[s], recv_sem=prx.at[s],
            device_id={"tp": partner}, device_id_type=MESH,
        )

    def fwd_copy(d, s, ck):
        b = order[2 * d]
        return pltpu.make_async_remote_copy(
            src_ref=xs.at[b, s, :, cols(ck)], dst_ref=xs.at[b, s, :, cols(ck)],
            send_sem=fwd_sem.at[d - 1, s, ck], recv_sem=rx.at[b, s, ck],
            device_id={"tp": partner}, device_id_type=MESH,
        )

    def arrive(b, s, ck):
        pltpu.make_async_remote_copy(
            src_ref=xs.at[b, s, :, cols(ck)], dst_ref=xs.at[b, s, :, cols(ck)],
            send_sem=part_sem.at[0], recv_sem=rx.at[b, s, ck],
            device_id={"tp": partner}, device_id_type=MESH,
        ).wait_recv()

    for s in range(seqs):
        for ck in range(chunks):
            token_copy(s, ck).wait()
            for d in range(1, chips):
                cross_copy(d, s, ck).start()
        part_copy(s).start()

    def small(x, start, depth, s, first):
        piece = bd[:, pl.ds(pl.multiple_of(start, depth), depth)]
        term = dot(piece, x, NT)
        sacc[s] = term if first else sacc[s] + term

    def use_whole(slot, s):
        b = order[slot]
        x = xs[b, s]
        for w in range(4):
            if s == 0:
                weight_copy(w, slot).wait()
            term = dot(x, wbuf[w, slot])
            acc[s, w] = term if slot == 0 else acc[s, w] + term
        small(x, b * kd, kd, s, slot == 0)

    def use(slot, s, ck):
        b = order[slot]
        x = xs[b, s, :, cols(ck)]
        for w in range(4):
            if s == 0 and ck == 0:
                weight_copy(w, slot).wait()
            acc[s, w] += dot(x, wbuf[w, slot, cols(ck), :])
        small(x, b * kd + ck * kc, kc, s, False)

    def forward(d, s, ck):
        arrive(order[2 * d], s, ck)
        fwd_copy(d, s, ck).start()

    def finish_chunk(d, s, ck):
        use(2 * d, s, ck)
        arrive(order[2 * d + 1], s, ck)
        use(2 * d + 1, s, ck)

    def heads_of(w, s):
        return [acc[s, w, :, h * extent : (h + 1) * extent].astype(bf16).astype(f32) for h in range(heads)]

    def owner_of(s, h):
        return (s * heads + h) % g

    def box_copy(s, h):
        return pltpu.make_async_remote_copy(
            src_ref=out_box.at[s, h], dst_ref=in_box.at[s, m],
            send_sem=send1.at[s, h], recv_sem=recv1.at[s, m],
            device_id={"sp": team * g + owner_of(s, h)}, device_id_type=MESH,
        )

    def boxes(s):
        beta = jax.nn.sigmoid(sacc[s, 0:PAD, :] + bias)
        pre = sacc[s, PAD : 2 * PAD, :]
        soft = jnp.maximum(pre, 0.0) + jnp.log1p(jnp.exp(-jnp.abs(pre)))
        upper = jnp.where(row <= col, 1.0, 0.0)
        cum = dot(-jnp.exp(rate) * soft, upper, NN, highest)
        cum_t, beta_t = cum.T, beta.T
        cum_col[s] = cum_t
        causal = row >= col
        strict = row > col
        unit = jnp.where(row == col, 1.0, 0.0)
        hs = range(heads)
        k = [unit_rows(v) for v in heads_of(1, s)]
        kh = [v.astype(bf16) for v in k]
        kk = [dot(v, v, NT) for v in kh]
        low, right, kdec, last = [], [], [], []
        v = heads_of(2, s)
        for h in hs:
            cumc, bt = cum_t[:, h : h + 1], beta_t[:, h : h + 1]
            wts = jnp.where(causal, jnp.exp(jnp.where(causal, cumc - cum[h : h + 1, :], 0.0)), 0.0)
            spread[h] = wts
            kh_buf[h] = kh[h]
            low.append(jnp.where(strict, kk[h] * (bt * wts), 0.0).astype(bf16))
            kb = k[h] * bt
            right.append(jnp.concatenate([v[h] * bt, kb * jnp.exp(cumc)], axis=1).astype(bf16))
            end = cumc[span - 1 :, :]
            kdec.append((k[h] * jnp.exp(end - cumc)).astype(bf16))
            last.append(jnp.exp(end))

        def climb(part, inv, size, ratio):
            if inv is None:
                power = part
                total = [unit - p.astype(f32) for p in part]
            else:
                low_h = [i.astype(bf16) for i in inv]
                power = [dot(i, p).astype(bf16) for i, p in zip(low_h, part)]
                total = [i - dot(p, j) for i, p, j in zip(inv, power, low_h)]
            reached = 2
            while reached < ratio:
                power = [dot(p, p).astype(bf16) for p in power]
                total = [t + dot(p, t.astype(bf16)) for t, p in zip(total, power)]
                reached *= 2
            return total

        inv = climb([p * masks[0] for p in low], None, INNER, INNER)
        inv = climb([p * masks[1] for p in low], inv, OUTER, OUTER // INNER)
        inv_h = [i.astype(bf16) for i in inv]
        power = [dot(i, p * masks[2]).astype(bf16) for i, p in zip(inv_h, low)]
        term = [dot(i, r) for i, r in zip(inv_h, right)]
        uw = term
        for level in range(1, -(-span // OUTER)):
            term = [dot(p, t.astype(bf16)) for p, t in zip(power, term)]
            uw = [u - t if level % 2 else u + t for u, t in zip(uw, term)]
        uw = [u.astype(bf16) for u in uw]
        z = [dot(a, u, TN) for a, u in zip(kdec, uw)]
        eye = lax.broadcasted_iota(jnp.int32, (extent, extent), 0) == lax.broadcasted_iota(
            jnp.int32, (extent, extent), 1
        )
        for h in hs:
            out_box[s, h, 0] = (jnp.where(eye, last[h] - 1.0, 0.0) - z[h][:, extent:]).astype(bf16)
            out_box[s, h, 1] = z[h][:, :extent].astype(bf16)
            uw_buf[h] = uw[h]
        for h in hs:
            own = m == owner_of(s, h)

            @pl.when(own)
            def _():
                in_box[s, m] = out_box[s, h]

            @pl.when(jnp.logical_not(own))
            def _():
                box_copy(s, h).start()

    def queries(s):
        cum_t = cum_col[s]
        gain = gain_ref[...]
        hs = range(heads)
        q = [unit_rows(v) for v in heads_of(0, s)]
        scores = [(dot(q[h].astype(bf16), kh_buf[h], NT) * spread[h]).astype(bf16) for h in hs]
        out = [dot(scores[h], uw_buf[h]) for h in hs]
        gates = heads_of(3, s)
        for h in hs:
            local_out[s, h] = out[h][:, :extent]
            reach[s, h] = (q[h] * jnp.exp(cum_t[:, h : h + 1]) - out[h][:, extent:]).astype(bf16)
            gated[s, h] = gates[h] * jax.nn.sigmoid(gates[h]) * gain

    def own_head(s):
        return lax.rem(m + g - (s * heads) % g, g)

    def back_copy(s, i):
        return pltpu.make_async_remote_copy(
            src_ref=back_out.at[s, i], dst_ref=back_in.at[s, own_head(s)],
            send_sem=send2.at[s, i], recv_sem=recv2.at[s, own_head(s)],
            device_id={"sp": team * g + i}, device_id_type=MESH,
        )

    def mid_copy(s):
        return pltpu.make_async_remote_copy(
            src_ref=mid_out.at[s], dst_ref=mid_in.at[s], send_sem=send3.at[s], recv_sem=recv3.at[s],
            device_id={"sp": lax.rem(me + g, sn)}, device_id_type=MESH,
        )

    def tail_copy(s, j):
        return pltpu.make_async_remote_copy(
            src_ref=tail_out.at[s, j], dst_ref=tail_in.at[s, own_head(s)],
            send_sem=send4.at[s, j], recv_sem=recv4.at[s, own_head(s)],
            device_id={"sp": j}, device_id_type=MESH,
        )

    def box_wait(s, i):
        @pl.when(i != m)
        def _():
            pltpu.make_async_remote_copy(
                src_ref=out_box.at[s, 0], dst_ref=in_box.at[s, i],
                send_sem=send1.at[s, 0], recv_sem=recv1.at[s, i],
                device_id={"sp": team * g + i}, device_id_type=MESH,
            ).wait_recv()

    def give_back(s):
        for i in range(g):

            @pl.when(i == m)
            def _():
                back_in[s, own_head(s)] = back_out[s, i]

            @pl.when(i != m)
            def _():
                back_copy(s, i).start()

    def conclude(s, final):
        memory = final.astype(bf16).astype(f32)
        h = own_head(s)
        shape3 = nq_ref.shape
        mine = (lax.broadcasted_iota(jnp.int32, shape3, 0) == s) & (lax.broadcasted_iota(jnp.int32, shape3, 1) == h)

        def own(ref):
            kept = jnp.where(mine, ref[...].astype(f32), 0.0)
            return jnp.sum(jnp.sum(kept, axis=0), axis=0, keepdims=True)

        qn, kn = unit_rows(own(nq_ref)), unit_rows(own(nk_ref))
        both = jnp.concatenate([jnp.broadcast_to(qn, (PAD, extent)), jnp.broadcast_to(kn, (PAD, extent))], axis=0)
        reads = dot(both, memory, NN, highest)
        recall, retrieve = reads[0:1], reads[PAD : PAD + 1]
        beta_new, decay_new = nb_ref[s, h], nd_ref[s, h]
        fresh = own(nv_ref) - decay_new * retrieve
        meet = jnp.sum(kn * qn, axis=-1, keepdims=True)
        read = decay_new * recall + (beta_new * meet) * fresh
        norm = lax.rsqrt(jnp.mean(read * read, axis=-1, keepdims=True) + norm_floor)
        answer = jnp.broadcast_to(read * norm * gain_ref[...], (PAD, extent))
        for j in range(sn):
            tail_out[s, j, 0:key_rows, :] = memory[j * key_rows : (j + 1) * key_rows]
            tail_out[s, j, tail_out.shape[2] - PAD :, :] = answer

        def push(j, _):
            @pl.when(j == me)
            def _():
                tail_in[s, h] = tail_out[s, me]

            @pl.when(j != me)
            def _():
                tail_copy(s, j).start()

            return 0

        lax.fori_loop(0, sn, push, 0)

    def chain_first(s):
        @pl.when((own_head(s) < heads) & (team == 0))
        def _():
            for i in range(g):
                box_wait(s, i)
            state = jnp.zeros((extent, extent), f32)
            for i in range(g):
                half = state.astype(bf16)
                back_out[s, i] = half
                if i == 0:
                    state = in_box[s, i, 1].astype(f32)
                else:
                    state = state + dot(in_box[s, i, 0], half) + in_box[s, i, 1].astype(f32)
            if groups > 1:
                mid_out[s] = state.astype(bf16)
                mid_copy(s).start()
            give_back(s)
            if groups == 1:
                conclude(s, state)

    def chain_later(s):
        if groups == 1:
            return

        @pl.when((own_head(s) < heads) & (team > 0))
        def _():
            for i in range(g):
                box_wait(s, i)
            shift, drive = [None], [None]
            for i in range(g):
                step, push = in_box[s, i, 0], in_box[s, i, 1].astype(f32)
                if i == 0:
                    shift.append(step.astype(f32))
                    drive.append(push)
                else:
                    shift.append(shift[i] + step.astype(f32) + dot(step, shift[i].astype(bf16)))
                    drive.append(drive[i] + push + dot(step, drive[i].astype(bf16)))
            moves = jnp.concatenate([a.astype(bf16) for a in shift[1:]], axis=0)
            pltpu.make_async_remote_copy(
                src_ref=mid_out.at[s], dst_ref=mid_in.at[s], send_sem=send3.at[s], recv_sem=recv3.at[s],
                device_id={"sp": lax.rem(me + sn - g, sn)}, device_id_type=MESH,
            ).wait_recv()
            start = mid_in[s]
            moved = dot(moves, start)
            base = start.astype(f32)
            back_out[s, 0] = start
            for i in range(1, g):
                back_out[s, i] = (base + moved[(i - 1) * extent : i * extent] + drive[i]).astype(bf16)
            state = base + moved[(g - 1) * extent :] + drive[g]

            @pl.when(team < groups - 1)
            def _():
                mid_out[s] = state.astype(bf16)
                mid_copy(s).start()

            give_back(s)

            @pl.when(team == groups - 1)
            def _():
                conclude(s, state)

    def finish(s):
        for h in range(heads):
            o = owner_of(s, h)

            @pl.when(m != o)
            def _():
                pltpu.make_async_remote_copy(
                    src_ref=back_out.at[s, 0], dst_ref=back_in.at[s, h],
                    send_sem=send2.at[s, 0], recv_sem=recv2.at[s, h],
                    device_id={"sp": team * g + o}, device_id_type=MESH,
                ).wait_recv()

        outs = [local_out[s, h] + dot(reach[s, h], back_in[s, h]) for h in range(heads)]
        for h in range(heads):
            o = outs[h]
            norm = lax.rsqrt(jnp.mean(o * o, axis=-1, keepdims=True) + norm_floor)
            mixed_ref[s * span : (s + 1) * span, h * extent : (h + 1) * extent] = (o * norm * gated[s, h]).astype(bf16)

    def take_tail(s):
        for h in range(heads):
            source = (groups - 1) * g + owner_of(s, h)

            @pl.when(me != source)
            def _():
                pltpu.make_async_remote_copy(
                    src_ref=tail_out.at[s, 0], dst_ref=tail_in.at[s, h],
                    send_sem=send4.at[s, 0], recv_sem=recv4.at[s, h],
                    device_id={"sp": source}, device_id_type=MESH,
                ).wait_recv()

            p = s * heads + h
            cache_ref[p] = tail_in[s, h, 0:key_rows, :].astype(bf16)
            edge = tail_in.shape[2] - PAD
            first_ref[p : p + 1, :] = tail_in[s, h, edge : edge + 1, :]

    for s in range(seqs):
        use_whole(0, s)
    for s in range(seqs):
        pltpu.make_async_remote_copy(
            src_ref=xs.at[partner, s], dst_ref=xs.at[partner, s], send_sem=part_sem.at[s], recv_sem=prx.at[s],
            device_id={"tp": partner}, device_id_type=MESH,
        ).wait_recv()
        use_whole(1, s)

    for s in range(seqs):
        for ck in range(chunks):
            for d in range(1, chips):
                if s == 0 or ck > 0:
                    forward(d, s, ck)
                if s > 0 and ck == chunks - 1 and d == chips - 1:
                    chain_first(s - 1)
                finish_chunk(d, s, ck)
        boxes(s)
        if s > 0:
            chain_later(s - 1)
        if s < seqs - 1:
            for d in range(1, chips):
                forward(d, s + 1, 0)
        queries(s)
    for s in range(seqs - 1):
        finish(s)
        take_tail(s)
    chain_first(seqs - 1)
    chain_later(seqs - 1)
    finish(seqs - 1)
    take_tail(seqs - 1)

    for s in range(seqs):
        part_copy(s).wait_send()
        for ck in range(chunks):
            for d in range(1, chips):
                cross_copy(d, s, ck).wait_send()
                fwd_copy(d, s, ck).wait_send()
        for h in range(heads):

            @pl.when(m != owner_of(s, h))
            def _():
                box_copy(s, h).wait_send()

        @pl.when(own_head(s) < heads)
        def _():
            for i in range(g):

                @pl.when(i != m)
                def _():
                    back_copy(s, i).wait_send()

            @pl.when(team < groups - 1)
            def _():
                mid_copy(s).wait_send()

            @pl.when(team == groups - 1)
            def _():
                for j in range(sn):

                    @pl.when(j != me)
                    def _():
                        tail_copy(s, j).wait_send()


def fused(tn, sn, seqs, heads, tokens, weights, bw, dw, bias, rate, gain, nq, nk, nv, nb, nd):
    rows, kd = tokens.shape
    width = weights[0].shape[1]
    kc = 256 if kd % 256 == 0 else kd
    chunks, chips, span = kd // kc, tn // 2, rows // seqs
    extent = width // heads
    pairs, key_rows = seqs * heads, extent // sn
    tail = -(-key_rows // PAD) * PAD + PAD
    g = group_of(sn, heads)
    vmem = pl.BlockSpec(memory_space=pltpu.VMEM)
    smem = pl.BlockSpec(memory_space=pltpu.SMEM)
    hbm = pl.BlockSpec(memory_space=pl.ANY)
    dma = pltpu.SemaphoreType.DMA
    return pl.pallas_call(
        functools.partial(fused_kernel, tn, sn, seqs, heads),
        out_shape=(
            jax.ShapeDtypeStruct((rows, width), bf16),
            jax.ShapeDtypeStruct((pairs, key_rows, extent), bf16),
            jax.ShapeDtypeStruct((pairs, extent), f32),
        ),
        in_specs=[hbm] * 5 + [vmem] * 2 + [smem] * 2 + [vmem] * 4 + [smem] * 2,
        out_specs=(vmem,) * 3,
        scratch_shapes=[
            pltpu.VMEM((2 * PAD, bw.shape[1]), bf16),
            pltpu.VMEM((tn, seqs, span, kd), bf16),
            pltpu.VMEM((4, tn, kd, width), bf16),
            pltpu.VMEM((seqs, 4, span, width), f32),
            pltpu.VMEM((seqs, 2 * PAD, span), f32),
            pltpu.VMEM((3, span, span), bf16),
            pltpu.VMEM((seqs, span, PAD), f32),
            pltpu.VMEM((heads, span, extent), bf16),
            pltpu.VMEM((heads, span, span), f32),
            pltpu.VMEM((heads, span, 2 * extent), bf16),
            pltpu.VMEM((seqs, heads, span, extent), f32),
            pltpu.VMEM((seqs, heads, span, extent), bf16),
            pltpu.VMEM((seqs, heads, span, extent), f32),
            pltpu.VMEM((seqs, heads, 2, extent, extent), bf16),
            pltpu.VMEM((seqs, g, 2, extent, extent), bf16),
            pltpu.VMEM((seqs, extent, extent), bf16),
            pltpu.VMEM((seqs, extent, extent), bf16),
            pltpu.VMEM((seqs, g, extent, extent), bf16),
            pltpu.VMEM((seqs, heads, extent, extent), bf16),
            pltpu.VMEM((seqs, sn, tail, extent), f32),
            pltpu.VMEM((seqs, heads, tail, extent), f32),
            dma((seqs, chunks)),
            dma((4, tn)),
            dma((chips - 1, seqs, chunks)),
            dma((seqs,)),
            dma((chips - 1, seqs, chunks)),
            dma((tn, seqs, chunks)),
            dma((seqs,)),
            dma((seqs, heads)),
            dma((seqs, g)),
            dma((seqs, g)),
            dma((seqs, heads)),
            dma((seqs,)),
            dma((seqs,)),
            dma((seqs, sn)),
            dma((seqs, heads)),
        ],
        compiler_params=pltpu.CompilerParams(
            collective_id=0, has_side_effects=True, vmem_limit_bytes=60 * 1024 * 1024
        ),
    )(tokens, *weights, bw, dw, bias, rate, gain, nq, nk, nv, nb, nd)


def shards(
    tokens, query_weight, key_weight, value_weight, gate_weight, beta_weight, decay_weight,
    beta_bias, rate_log, out_gain, new_query, new_key, new_value, new_beta, new_decay,
):
    seqs, span, kd = tokens.shape
    heads = rate_log.shape[0]
    extent = out_gain.shape[0]
    tp, sp = lax.axis_size("tp"), lax.axis_size("sp")
    weights = (query_weight, key_weight, value_weight, gate_weight)
    mixed, cache, first = fused(
        tp, sp, seqs, heads, tokens.reshape(seqs * span, kd), weights, beta_weight.T, decay_weight.T, beta_bias,
        rate_log, out_gain[None], new_query, new_key, new_value, new_beta, new_decay,
    )
    return (
        mixed.reshape(seqs, span, heads * extent),
        cache.reshape(seqs, heads, extent // sp, extent),
        first.reshape(seqs, heads * extent),
    )


def solution(mesh):
    placed = (
        P(None, "sp", "tp"),
        P(None, "tp"),
        P(None, "tp"),
        P(None, "tp"),
        P(None, "tp"),
        P(None, "tp"),
        P(None, "tp"),
        P("tp"),
        P("tp"),
        P(),
        P(None, "tp", None),
        P(None, "tp", None),
        P(None, "tp", None),
        P(None, "tp"),
        P(None, "tp"),
    )
    return jax.shard_map(
        shards,
        mesh=mesh,
        in_specs=placed,
        out_specs=(P(None, "sp", "tp"), P(None, "tp", "sp", None), P(None, "tp")),
        check_vma=False,
    )
```

time: 62.3 us -> 56.4 us (0.905)
  Pallas kernels: 56.8 us -> 51 us
    pallas_call x2 -> x1, Pallas kernels: 56.8 us -> 51 us  [fused(): pl.pallas_call(functools.partial(fused_kernel, tn, sn, seqs, heads), out_...]
    reshape x1, local copies, waits for them, and re-layouts: 0.6 us -> 1.28 us  [shards(): first.reshape(seqs, heads * extent)]
    unnamed x22 -> x2, local copies, waits for them, and re-layouts: 3.55 us -> 3.14 us
where the time goes in v1:
time: 56.4 us; the launch traced here: 56.1 us
  Pallas kernels  51 us (90%)
  local copies, waits for them, and re-layouts  4.42 us (8%)
  between operations  0.65 us (1%)
    pallas_call x1, Pallas kernels, fused(): pl.pallas_call(functools.partial(fused_kernel, tn, sn, seqs, heads), out_...  51 us
    unnamed x2, local copies, waits for them, and re-layouts  3.14 us
    reshape x1, local copies, waits for them, and re-layouts, shards(): first.reshape(seqs, heads * extent)  1.28 us

profile of v1, /device:TPU:0, one launch (start us, length us, event | category | flops | bytes accessed | tf_op | source)
XLA Modules:
  0.0 56.1 jit_solution(6536050368463879077)
XLA Ops:
  0.6 51.0 %shard_map.166 = (bf16[384,512]{1,0:T(8,128)(2,1)}, bf16[8,16,128]{2,1,0:T(8,128)(2,1)}, f32[8,128]{1,0:T(8,128)}) custom-call(bf16[384,1024]{1,0:T(8,128)(2,1)} %bitcast.6, bf16[4096,512]{1,0:T(8,128)(2,1)} %wq_ref.1, bf16[4096,512]{1,0:T(8,128)(2,1)} %wk_ref.1, bf16[4096,512]{1,0:T(8,128)(2,1)} %wv_ref.1, bf16[4096,512]{1,0:T(8,128)(2,1)} %wg_ref.1, ...), custom_call_target="tpu_custom_call" | custom-call | tf_op jit(solution)/shard_map/pallas_call | solution.py:537
  51.7 1.3 %reshape.21 = f32[2,512]{1,0:T(2,128)} reshape(f32[8,128]{1,0:T(8,128)} %get-tuple-element.8) | data formatting | bytes 8192 | tf_op jit(solution)/shard_map/reshape | solution.py:606
  53.0 1.8 %copy.20 = bf16[2,192,512]{2,1,0:T(8,128)(2,1)} copy(bf16[2,192,512]{2,1,0:T(8,128)(2,1)} %bitcast.7) | data formatting | bytes 786432
  54.7 1.4 %copy.21 = bf16[2,4,16,128]{3,2,1,0:T(8,128)(2,1)} copy(bf16[2,4,16,128]{3,2,1,0:T(8,128)(2,1)} %bitcast.10) | data formatting | bytes 65536

commit v2 on v1

--- a/solution.py
+++ b/solution.py
@@ -42,13 +42,13 @@
     bd, xs, wbuf, acc, sacc, masks, cum_col, kh_buf, spread, uw_buf, local_out, reach, gated,
     out_box, in_box, mid_out, mid_in, back_out, back_in, tail_out, tail_in,
     xsem, wsem, cross_sem, part_sem, fwd_sem, rx, prx,
-    send1, recv1, send2, recv2, send3, recv3, send4, recv4,
+    send1, recv1, send2, recv2, send3, recv3, send4, recv4, hello,
 ):
     _, _, span, kd = xs.shape
     width = wq_ref.shape[1]
     extent = width // heads
     key_rows = extent // sn
-    chunks = xsem.shape[1]
+    chunks = rx.shape[2]
     kc = kd // chunks
     tme, me = lax.axis_index("tp"), lax.axis_index("sp")
     y, c = tme // 2, lax.rem(tme, 2)
@@ -65,7 +65,10 @@
         to = lax.rem(y + d, chips) * 2 + c
         pl.semaphore_signal(barrier, inc=1, device_id={"tp": to}, device_id_type=MESH)
     for d in range(1, sn):
-        pl.semaphore_signal(barrier, inc=1, device_id={"sp": lax.rem(me + d, sn)}, device_id_type=MESH)
+
+        @pl.when(me + d < sn)
+        def _():
+            pl.semaphore_signal(barrier, inc=1, device_id={"sp": me + d}, device_id_type=MESH)
 
     order = [tme, partner]
     for d in range(1, chips):
@@ -75,10 +78,8 @@
     def cols(ck):
         return pl.ds(ck * kc, kc)
 
-    def token_copy(s, ck):
-        return pltpu.make_async_copy(
-            x_ref.at[pl.ds(s * span, span), cols(ck)], xs.at[tme, s, :, cols(ck)], xsem.at[s, ck]
-        )
+    def token_copy(s):
+        return pltpu.make_async_copy(x_ref.at[pl.ds(s * span, span), :], xs.at[tme, s], xsem.at[s])
 
     def weight_copy(w, slot):
         start = pl.multiple_of(order[slot] * kd, kd)
@@ -87,11 +88,38 @@
         )
 
     for s in range(seqs):
+        token_copy(s).start()
+    pl.semaphore_wait(barrier, chips + me)
+
+    def cross_copy(d, s, ck):
+        to = lax.rem(y + d, chips) * 2 + c
+        return pltpu.make_async_remote_copy(
+            src_ref=xs.at[tme, s, :, cols(ck)], dst_ref=xs.at[tme, s, :, cols(ck)],
+            send_sem=cross_sem.at[d - 1, s, ck], recv_sem=rx.at[tme, s, ck],
+            device_id={"tp": to}, device_id_type=MESH,
+        )
+
+    def part_copy(s):
+        return pltpu.make_async_remote_copy(
+            src_ref=xs.at[tme, s], dst_ref=xs.at[tme, s],
+            send_sem=part_sem.at[s], recv_sem=prx.at[s],
+            device_id={"tp": partner}, device_id_type=MESH,
+        )
+
+    for s in range(seqs):
+        token_copy(s).wait()
         for ck in range(chunks):
-            token_copy(s, ck).start()
+            for d in range(1, chips):
+                cross_copy(d, s, ck).start()
+        part_copy(s).start()
     for slot in range(tn):
         for w in range(4):
             weight_copy(w, slot).start()
+    for d in range(1, sn):
+
+        @pl.when(me >= d)
+        def _():
+            pl.semaphore_signal(hello, inc=1, device_id={"sp": me - d}, device_id_type=MESH)
 
     bd[...] = jnp.zeros_like(bd)
     bd[0 : bw_ref.shape[0]] = bw_ref[...]
@@ -109,22 +137,6 @@
     for h in range(heads):
         bias = jnp.where(slot_of == h, bias_ref[h], bias)
         rate = jnp.where(slot_of == h, rate_ref[h], rate)
-    pl.semaphore_wait(barrier, chips + sn - 1)
-
-    def cross_copy(d, s, ck):
-        to = lax.rem(y + d, chips) * 2 + c
-        return pltpu.make_async_remote_copy(
-            src_ref=xs.at[tme, s, :, cols(ck)], dst_ref=xs.at[tme, s, :, cols(ck)],
-            send_sem=cross_sem.at[d - 1, s, ck], recv_sem=rx.at[tme, s, ck],
-            device_id={"tp": to}, device_id_type=MESH,
-        )
-
-    def part_copy(s):
-        return pltpu.make_async_remote_copy(
-            src_ref=xs.at[tme, s], dst_ref=xs.at[tme, s],
-            send_sem=part_sem.at[s], recv_sem=prx.at[s],
-            device_id={"tp": partner}, device_id_type=MESH,
-        )
 
     def fwd_copy(d, s, ck):
         b = order[2 * d]
@@ -140,13 +152,6 @@
             send_sem=part_sem.at[0], recv_sem=rx.at[b, s, ck],
             device_id={"tp": partner}, device_id_type=MESH,
         ).wait_recv()
-
-    for s in range(seqs):
-        for ck in range(chunks):
-            token_copy(s, ck).wait()
-            for d in range(1, chips):
-                cross_copy(d, s, ck).start()
-        part_copy(s).start()
 
     def small(x, start, depth, s, first):
         piece = bd[:, pl.ds(pl.multiple_of(start, depth), depth)]
@@ -256,6 +261,12 @@
             out_box[s, h, 0] = (jnp.where(eye, last[h] - 1.0, 0.0) - z[h][:, extent:]).astype(bf16)
             out_box[s, h, 1] = z[h][:, :extent].astype(bf16)
             uw_buf[h] = uw[h]
+        if s == 0:
+
+            @pl.when(me < sn - 1)
+            def _():
+                pl.semaphore_wait(hello, sn - 1 - me)
+
         for h in hs:
             own = m == owner_of(s, h)
 
@@ -454,7 +465,7 @@
             p = s * heads + h
             cache_ref[p] = tail_in[s, h, 0:key_rows, :].astype(bf16)
             edge = tail_in.shape[2] - PAD
-            first_ref[p : p + 1, :] = tail_in[s, h, edge : edge + 1, :]
+            first_ref[s : s + 1, h * extent : (h + 1) * extent] = tail_in[s, h, edge : edge + 1, :]
 
     for s in range(seqs):
         use_whole(0, s)
@@ -482,11 +493,11 @@
         queries(s)
     for s in range(seqs - 1):
         finish(s)
-        take_tail(s)
     chain_first(seqs - 1)
     chain_later(seqs - 1)
     finish(seqs - 1)
-    take_tail(seqs - 1)
+    for s in range(seqs):
+        take_tail(s)
 
     for s in range(seqs):
         part_copy(s).wait_send()
@@ -530,16 +541,17 @@
     pairs, key_rows = seqs * heads, extent // sn
     tail = -(-key_rows // PAD) * PAD + PAD
     g = group_of(sn, heads)
+    operands = (tokens, *weights, bw, dw, bias, rate, gain, nq, nk, nv, nb, nd)
     vmem = pl.BlockSpec(memory_space=pltpu.VMEM)
     smem = pl.BlockSpec(memory_space=pltpu.SMEM)
-    hbm = pl.BlockSpec(memory_space=pl.ANY)
+    hbm = pl.BlockSpec(memory_space=pltpu.HBM)
     dma = pltpu.SemaphoreType.DMA
     return pl.pallas_call(
         functools.partial(fused_kernel, tn, sn, seqs, heads),
         out_shape=(
             jax.ShapeDtypeStruct((rows, width), bf16),
             jax.ShapeDtypeStruct((pairs, key_rows, extent), bf16),
-            jax.ShapeDtypeStruct((pairs, extent), f32),
+            jax.ShapeDtypeStruct((seqs, width), f32),
         ),
         in_specs=[hbm] * 5 + [vmem] * 2 + [smem] * 2 + [vmem] * 4 + [smem] * 2,
         out_specs=(vmem,) * 3,
@@ -565,7 +577,7 @@
             pltpu.VMEM((seqs, heads, extent, extent), bf16),
             pltpu.VMEM((seqs, sn, tail, extent), f32),
             pltpu.VMEM((seqs, heads, tail, extent), f32),
-            dma((seqs, chunks)),
+            dma((seqs,)),
             dma((4, tn)),
             dma((chips - 1, seqs, chunks)),
             dma((seqs,)),
@@ -580,11 +592,34 @@
             dma((seqs,)),
             dma((seqs, sn)),
             dma((seqs, heads)),
+            pltpu.SemaphoreType.REGULAR,
         ],
         compiler_params=pltpu.CompilerParams(
-            collective_id=0, has_side_effects=True, vmem_limit_bytes=60 * 1024 * 1024
+            collective_id=0, has_side_effects=True, vmem_limit_bytes=53 * 1024 * 1024
         ),
-    )(tokens, *weights, bw, dw, bias, rate, gain, nq, nk, nv, nb, nd)
+    )(*[pltpu.with_memory_space_constraint(a, pltpu.HBM) for a in operands])
+
+
+def emit_kernel(mixed_ref, cache_ref, first_ref, mixed_out, cache_out, first_out, sem):
+    copies = [
+        pltpu.make_async_copy(a, b, sem.at[i])
+        for i, (a, b) in enumerate(((mixed_ref, mixed_out), (cache_ref, cache_out), (first_ref, first_out)))
+    ]
+    for copy in copies:
+        copy.start()
+    for copy in copies:
+        copy.wait()
+
+
+def emit(*results):
+    return pl.pallas_call(
+        emit_kernel,
+        out_shape=tuple(jax.ShapeDtypeStruct(r.shape, r.dtype) for r in results),
+        in_specs=[pl.BlockSpec(memory_space=pltpu.VMEM)] * 3,
+        out_specs=(pl.BlockSpec(memory_space=pltpu.HBM),) * 3,
+        scratch_shapes=[pltpu.SemaphoreType.DMA((3,))],
+        compiler_params=pltpu.CompilerParams(vmem_limit_bytes=4 * 1024 * 1024),
+    )(*results)
 
 
 def shards(
@@ -600,10 +635,8 @@
         tp, sp, seqs, heads, tokens.reshape(seqs * span, kd), weights, beta_weight.T, decay_weight.T, beta_bias,
         rate_log, out_gain[None], new_query, new_key, new_value, new_beta, new_decay,
     )
-    return (
-        mixed.reshape(seqs, span, heads * extent),
-        cache.reshape(seqs, heads, extent // sp, extent),
-        first.reshape(seqs, heads * extent),
+    return emit(
+        mixed.reshape(seqs, span, heads * extent), cache.reshape(seqs, heads, extent // sp, extent), first
     )
 
 

time: 56.4 us -> 46.1 us (0.82)
  Pallas kernels: 51 us -> 45.2 us
  local copies, waits for them, and re-layouts: 4.42 us -> 0 us
    pallas_call x1, Pallas kernels: 51 us -> 44.4 us  [fused(): pl.pallas_call(functools.partial(fused_kernel, tn, sn, seqs, heads), out_...]
    unnamed x2 -> x0, local copies, waits for them, and re-layouts: 3.14 us -> none
    reshape x1 -> x0, local copies, waits for them, and re-layouts: 1.28 us -> none  [shards(): first.reshape(seqs, heads * extent)]
    pallas_call x0 -> x1, Pallas kernels: none -> 0.78 us  [emit(): pl.pallas_call(emit_kernel, out_shape=tuple((jax.ShapeDtypeStruct(r.shape...]
where the time goes in v2:
time: 46.1 us; the launch traced here: 46 us
  Pallas kernels  45.2 us (98%)
  between operations  0.81 us (2%)
    pallas_call x1, Pallas kernels, fused(): pl.pallas_call(functools.partial(fused_kernel, tn, sn, seqs, heads), out_...  44.4 us

profile of v2, /device:TPU:0, one launch (start us, length us, event | category | flops | bytes accessed | tf_op | source)
XLA Modules:
  0.0 46.0 jit_solution(1257935218489537866)
XLA Ops:
  0.6 44.4 %shard_map.166 = (bf16[384,512]{1,0:T(8,128)(2,1)S(1)}, bf16[8,16,128]{2,1,0:T(8,128)(2,1)S(1)}, f32[2,512]{1,0:T(2,128)S(1)}) custom-call(bf16[384,1024]{1,0:T(8,128)(2,1)} %bitcast.8, bf16[4096,512]{1,0:T(8,128)(2,1)} %wq_ref.1, bf16[4096,512]{1,0:T(8,128)(2,1)} %wk_ref.1, bf16[4096,512]{1,0:T(8,128)(2,1)} %wv_ref.1, bf16[4096,512]{1,0:T(8,128)(2,1)} %wg_ref.1, ...), custom_call_target="tpu_custom_call" | custom-call | tf_op jit(solution)/shard_map/pallas_call | solution.py:549
  45.0 0.8 %shard_map.167 = (bf16[2,192,512]{2,1,0:T(8,128)(2,1)}, bf16[2,4,16,128]{3,2,1,0:T(8,128)(2,1)}, f32[2,512]{1,0:T(2,128)}) custom-call(bf16[2,192,512]{2,1,0:T(8,128)(2,1)S(1)} %bitcast.6, bf16[2,4,16,128]{3,2,1,0:T(8,128)(2,1)S(1)} %bitcast.7, f32[2,512]{1,0:T(2,128)S(1)} %get-tuple-element.8.first_ref), custom_call_target="tpu_custom_call" | custom-call | tf_op jit(solution)/shard_map/pallas_call | solution.py:615

commit v3 on v2

--- a/solution.py
+++ b/solution.py
@@ -37,12 +37,13 @@
 
 
 def fused_kernel(
-    tn, sn, seqs, heads, x_ref, wq_ref, wk_ref, wv_ref, wg_ref, bw_ref, dw_ref, bias_ref, rate_ref, gain_ref,
-    nq_ref, nk_ref, nv_ref, nb_ref, nd_ref, mixed_ref, cache_ref, first_ref,
-    bd, xs, wbuf, acc, sacc, masks, cum_col, kh_buf, spread, uw_buf, local_out, reach, gated,
-    out_box, in_box, mid_out, mid_in, back_out, back_in, tail_out, tail_in,
+    tn, sn, seqs, heads, x_ref, wq_ref, wk_ref, wv_ref, wg_ref, bw_hbm, dw_hbm, bias_hbm, rate_hbm, gain_hbm,
+    nq_hbm, nk_hbm, nv_hbm, nb_hbm, nd_hbm, mixed_ref, cache_ref, first_ref,
+    bw_ref, dw_ref, bias_ref, rate_ref, gain_ref, nq_ref, nk_ref, nv_ref, nb_ref, nd_ref, small_sem,
+    bd, xs, wbuf, acc, sacc, cum_row, cum_col, kh_buf, uw_buf, local_out, reach, gated,
+    out_box, in_box, mid_out, mid_in, back_out, back_in, tail_out, tail_in, word_out, word_in,
     xsem, wsem, cross_sem, part_sem, fwd_sem, rx, prx,
-    send1, recv1, send2, recv2, send3, recv3, send4, recv4, hello,
+    send1, recv1, send2, recv2, send3, recv3, send4, recv4, send5, recv5, hello,
 ):
     _, _, span, kd = xs.shape
     width = wq_ref.shape[1]
@@ -87,8 +88,19 @@
             weights[w].at[pl.ds(start, kd), :], wbuf.at[w, slot], wsem.at[w, slot]
         )
 
+    small_copies = [
+        pltpu.make_async_copy(a, b, small_sem.at[i])
+        for i, (a, b) in enumerate(
+            (
+                (bw_hbm, bw_ref), (dw_hbm, dw_ref), (bias_hbm, bias_ref), (rate_hbm, rate_ref), (gain_hbm, gain_ref),
+                (nq_hbm, nq_ref), (nk_hbm, nk_ref), (nv_hbm, nv_ref), (nb_hbm, nb_ref), (nd_hbm, nd_ref),
+            )
+        )
+    ]
     for s in range(seqs):
         token_copy(s).start()
+    for copy in small_copies:
+        copy.start()
     pl.semaphore_wait(barrier, chips + me)
 
     def cross_copy(d, s, ck):
@@ -121,16 +133,13 @@
         def _():
             pl.semaphore_signal(hello, inc=1, device_id={"sp": me - d}, device_id_type=MESH)
 
+    for copy in small_copies:
+        copy.wait()
     bd[...] = jnp.zeros_like(bd)
     bd[0 : bw_ref.shape[0]] = bw_ref[...]
     bd[PAD : PAD + dw_ref.shape[0]] = dw_ref[...]
     row = lax.broadcasted_iota(jnp.int32, (span, span), 0)
     col = lax.broadcasted_iota(jnp.int32, (span, span), 1)
-    same_in = row // INNER == col // INNER
-    same_out = row // OUTER == col // OUTER
-    masks[0] = jnp.where(same_in, 1.0, 0.0).astype(bf16)
-    masks[1] = jnp.where(same_out & ~same_in, 1.0, 0.0).astype(bf16)
-    masks[2] = jnp.where(same_out, 0.0, 1.0).astype(bf16)
     slot_of = lax.broadcasted_iota(jnp.int32, (PAD, 1), 0)
     bias = jnp.zeros((PAD, 1), f32)
     rate = jnp.zeros((PAD, 1), f32)
@@ -206,53 +215,74 @@
         upper = jnp.where(row <= col, 1.0, 0.0)
         cum = dot(-jnp.exp(rate) * soft, upper, NN, highest)
         cum_t, beta_t = cum.T, beta.T
+        cum_row[s] = cum
         cum_col[s] = cum_t
-        causal = row >= col
-        strict = row > col
-        unit = jnp.where(row == col, 1.0, 0.0)
-        hs = range(heads)
+        hs, bs = range(heads), range(span // OUTER)
+        line = lax.broadcasted_iota(jnp.int32, (OUTER, 2 * OUTER), 0)
+        lane = lax.broadcasted_iota(jnp.int32, (OUTER, 2 * OUTER), 1)
+        high = lane >= OUTER
+        place = lane % OUTER
+        same = line // INNER == place // INNER
+        fill = jnp.zeros((OUTER, 2 * OUTER), bf16)
+        unit = jnp.where(line == place, 1.0, 0.0)
+
+        def part(b):
+            return slice(b * OUTER, (b + 1) * OUTER)
+
+        twice = [jnp.concatenate([cum[:, part(b)]] * 2, axis=1) for b in bs]
         k = [unit_rows(v) for v in heads_of(1, s)]
         kh = [v.astype(bf16) for v in k]
-        kk = [dot(v, v, NT) for v in kh]
-        low, right, kdec, last = [], [], [], []
+        pairs = [(h, b) for h in hs for b in bs]
+        kk = [dot(kh[h][part(b)], jnp.concatenate([kh[h][part(b)]] * 2, axis=0), NT) for h, b in pairs]
+        far = {(h, b): dot(kh[h][part(b)], kh[h][: b * OUTER], NT) for h, b in pairs if b > 0}
+        right, kdec, last, low = [], [], [], []
         v = heads_of(2, s)
         for h in hs:
             cumc, bt = cum_t[:, h : h + 1], beta_t[:, h : h + 1]
-            wts = jnp.where(causal, jnp.exp(jnp.where(causal, cumc - cum[h : h + 1, :], 0.0)), 0.0)
-            spread[h] = wts
             kh_buf[h] = kh[h]
-            low.append(jnp.where(strict, kk[h] * (bt * wts), 0.0).astype(bf16))
+            for b in bs:
+                here = cumc[part(b)]
+                wts = bt[part(b)] * jnp.exp(jnp.where(line >= place, here - twice[b][h : h + 1, :], 0.0))
+                low.append(jnp.where(line > place, kk[h * len(bs) + b] * wts, 0.0))
+                if b > 0:
+                    wts = bt[part(b)] * jnp.exp(here - cum[h : h + 1, : b * OUTER])
+                    far[h, b] = (far[h, b] * wts).astype(bf16)
             kb = k[h] * bt
             right.append(jnp.concatenate([v[h] * bt, kb * jnp.exp(cumc)], axis=1).astype(bf16))
             end = cumc[span - 1 :, :]
             kdec.append((k[h] * jnp.exp(end - cumc)).astype(bf16))
             last.append(jnp.exp(end))
 
-        def climb(part, inv, size, ratio):
-            if inv is None:
-                power = part
-                total = [unit - p.astype(f32) for p in part]
-            else:
-                low_h = [i.astype(bf16) for i in inv]
-                power = [dot(i, p).astype(bf16) for i, p in zip(low_h, part)]
-                total = [i - dot(p, j) for i, p, j in zip(inv, power, low_h)]
-            reached = 2
-            while reached < ratio:
-                power = [dot(p, p).astype(bf16) for p in power]
-                total = [t + dot(p, t.astype(bf16)) for t, p in zip(total, power)]
-                reached *= 2
-            return total
-
-        inv = climb([p * masks[0] for p in low], None, INNER, INNER)
-        inv = climb([p * masks[1] for p in low], inv, OUTER, OUTER // INNER)
-        inv_h = [i.astype(bf16) for i in inv]
-        power = [dot(i, p * masks[2]).astype(bf16) for i, p in zip(inv_h, low)]
-        term = [dot(i, r) for i, r in zip(inv_h, right)]
-        uw = term
-        for level in range(1, -(-span // OUTER)):
-            term = [dot(p, t.astype(bf16)) for p, t in zip(power, term)]
-            uw = [u - t if level % 2 else u + t for u, t in zip(uw, term)]
-        uw = [u.astype(bf16) for u in uw]
+        def climb(block):
+            half = block.astype(bf16)
+            return dot(half[:, :OUTER], half)
+
+        z = [jnp.where(high, unit - n, n) for n in (jnp.where(same, m, 0.0) for m in low)]
+        z = [jnp.where(high, a, climb(a)) for a in z]
+        reached = 2
+        while reached < INNER:
+            z = [climb(a) + jnp.where(high, a, 0.0) for a in z]
+            reached *= 2
+        under = [jnp.concatenate([fill, jnp.where(high | same, 0.0, m).astype(bf16)], axis=0) for m in low]
+        z = [a + dot(a.astype(bf16), u) for a, u in zip(z, under)]
+        z = [jnp.where(high, a - t, t) for a, t in ((a, climb(a)) for a in z)]
+        reached = 2
+        while reached < OUTER // INNER:
+            z = [climb(a) + jnp.where(high, a, 0.0) for a in z]
+            reached *= 2
+        inv = {p: a.astype(bf16) for p, a in zip(pairs, z)}
+        none = jnp.zeros((OUTER, 2 * extent), bf16)
+        term = {(h, b): dot(inv[h, b], jnp.concatenate([none, right[h][part(b)]], axis=0)) for h, b in pairs}
+        far = {
+            (h, b): dot(inv[h, b], jnp.concatenate([jnp.zeros_like(m), m], axis=0)).astype(bf16)
+            for (h, b), m in far.items()
+        }
+        done = [[term[h, 0].astype(bf16)] for h in hs]
+        for b in bs[1:]:
+            for h in hs:
+                seen = jnp.concatenate(done[h], axis=0) if b > 1 else done[h][0]
+                done[h].append((term[h, b] - dot(far[h, b], seen)).astype(bf16))
+        uw = [jnp.concatenate(d, axis=0) for d in done]
         z = [dot(a, u, TN) for a, u in zip(kdec, uw)]
         eye = lax.broadcasted_iota(jnp.int32, (extent, extent), 0) == lax.broadcasted_iota(
             jnp.int32, (extent, extent), 1
@@ -279,11 +309,17 @@
                 box_copy(s, h).start()
 
     def queries(s):
-        cum_t = cum_col[s]
+        cum, cum_t = cum_row[s], cum_col[s]
         gain = gain_ref[...]
         hs = range(heads)
+        causal = row >= col
+
+        def spread(h):
+            gap = jnp.where(causal, cum_t[:, h : h + 1] - cum[h : h + 1, :], 0.0)
+            return jnp.where(causal, jnp.exp(gap), 0.0)
+
         q = [unit_rows(v) for v in heads_of(0, s)]
-        scores = [(dot(q[h].astype(bf16), kh_buf[h], NT) * spread[h]).astype(bf16) for h in hs]
+        scores = [(dot(q[h].astype(bf16), kh_buf[h], NT) * spread(h)).astype(bf16) for h in hs]
         out = [dot(scores[h], uw_buf[h]) for h in hs]
         gates = heads_of(3, s)
         for h in hs:
@@ -307,11 +343,17 @@
             device_id={"sp": lax.rem(me + g, sn)}, device_id_type=MESH,
         )
 
-    def tail_copy(s, j):
-        return pltpu.make_async_remote_copy(
-            src_ref=tail_out.at[s, j], dst_ref=tail_in.at[s, own_head(s)],
-            send_sem=send4.at[s, j], recv_sem=recv4.at[s, own_head(s)],
-            device_id={"sp": j}, device_id_type=MESH,
+    def tail_copies(s, j):
+        h = own_head(s)
+        return (
+            pltpu.make_async_remote_copy(
+                src_ref=tail_out.at[s, j], dst_ref=tail_in.at[s, h], send_sem=send4.at[s, j], recv_sem=recv4.at[s, h],
+                device_id={"sp": j}, device_id_type=MESH,
+            ),
+            pltpu.make_async_remote_copy(
+                src_ref=word_out.at[s], dst_ref=word_in.at[s, h], send_sem=send5.at[s, j], recv_sem=recv5.at[s, h],
+                device_id={"sp": j}, device_id_type=MESH,
+            ),
         )
 
     def box_wait(s, i):
@@ -335,8 +377,11 @@
                 back_copy(s, i).start()
 
     def conclude(s, final):
-        memory = final.astype(bf16).astype(f32)
+        kept_h = final.astype(bf16)
+        memory = kept_h.astype(f32)
         h = own_head(s)
+        for j in range(sn):
+            tail_out[s, j] = kept_h[j * key_rows : (j + 1) * key_rows]
         shape3 = nq_ref.shape
         mine = (lax.broadcasted_iota(jnp.int32, shape3, 0) == s) & (lax.broadcasted_iota(jnp.int32, shape3, 1) == h)
 
@@ -353,23 +398,18 @@
         meet = jnp.sum(kn * qn, axis=-1, keepdims=True)
         read = decay_new * recall + (beta_new * meet) * fresh
         norm = lax.rsqrt(jnp.mean(read * read, axis=-1, keepdims=True) + norm_floor)
-        answer = jnp.broadcast_to(read * norm * gain_ref[...], (PAD, extent))
+        word_out[s] = read * norm * gain_ref[...]
         for j in range(sn):
-            tail_out[s, j, 0:key_rows, :] = memory[j * key_rows : (j + 1) * key_rows]
-            tail_out[s, j, tail_out.shape[2] - PAD :, :] = answer
-
-        def push(j, _):
+
             @pl.when(j == me)
             def _():
-                tail_in[s, h] = tail_out[s, me]
+                tail_in[s, h] = tail_out[s, j]
+                word_in[s, h] = word_out[s]
 
             @pl.when(j != me)
             def _():
-                tail_copy(s, j).start()
-
-            return 0
-
-        lax.fori_loop(0, sn, push, 0)
+                for copy in tail_copies(s, j):
+                    copy.start()
 
     def chain_first(s):
         @pl.when((own_head(s) < heads) & (team == 0))
@@ -387,9 +427,9 @@
             if groups > 1:
                 mid_out[s] = state.astype(bf16)
                 mid_copy(s).start()
-            give_back(s)
             if groups == 1:
                 conclude(s, state)
+            give_back(s)
 
     def chain_later(s):
         if groups == 1:
@@ -426,11 +466,11 @@
                 mid_out[s] = state.astype(bf16)
                 mid_copy(s).start()
 
+            @pl.when(team == groups - 1)
+            def _():
+                conclude(s, state)
+
             give_back(s)
-
-            @pl.when(team == groups - 1)
-            def _():
-                conclude(s, state)
 
     def finish(s):
         for h in range(heads):
@@ -461,11 +501,14 @@
                     send_sem=send4.at[s, 0], recv_sem=recv4.at[s, h],
                     device_id={"sp": source}, device_id_type=MESH,
                 ).wait_recv()
-
-            p = s * heads + h
-            cache_ref[p] = tail_in[s, h, 0:key_rows, :].astype(bf16)
-            edge = tail_in.shape[2] - PAD
-            first_ref[s : s + 1, h * extent : (h + 1) * extent] = tail_in[s, h, edge : edge + 1, :]
+                pltpu.make_async_remote_copy(
+                    src_ref=word_out.at[s], dst_ref=word_in.at[s, h],
+                    send_sem=send5.at[s, 0], recv_sem=recv5.at[s, h],
+                    device_id={"sp": source}, device_id_type=MESH,
+                ).wait_recv()
+
+            cache_ref[s * heads + h] = tail_in[s, h]
+            first_ref[s : s + 1, h * extent : (h + 1) * extent] = word_in[s, h]
 
     for s in range(seqs):
         use_whole(0, s)
@@ -497,9 +540,6 @@
     chain_later(seqs - 1)
     finish(seqs - 1)
     for s in range(seqs):
-        take_tail(s)
-
-    for s in range(seqs):
         part_copy(s).wait_send()
         for ck in range(chunks):
             for d in range(1, chips):
@@ -529,7 +569,11 @@
 
                     @pl.when(j != me)
                     def _():
-                        tail_copy(s, j).wait_send()
+                        for copy in tail_copies(s, j):
+                            copy.wait_send()
+
+    for s in range(seqs):
+        take_tail(s)
 
 
 def fused(tn, sn, seqs, heads, tokens, weights, bw, dw, bias, rate, gain, nq, nk, nv, nb, nd):
@@ -539,11 +583,9 @@
     chunks, chips, span = kd // kc, tn // 2, rows // seqs
     extent = width // heads
     pairs, key_rows = seqs * heads, extent // sn
-    tail = -(-key_rows // PAD) * PAD + PAD
     g = group_of(sn, heads)
     operands = (tokens, *weights, bw, dw, bias, rate, gain, nq, nk, nv, nb, nd)
     vmem = pl.BlockSpec(memory_space=pltpu.VMEM)
-    smem = pl.BlockSpec(memory_space=pltpu.SMEM)
     hbm = pl.BlockSpec(memory_space=pltpu.HBM)
     dma = pltpu.SemaphoreType.DMA
     return pl.pallas_call(
@@ -553,18 +595,28 @@
             jax.ShapeDtypeStruct((pairs, key_rows, extent), bf16),
             jax.ShapeDtypeStruct((seqs, width), f32),
         ),
-        in_specs=[hbm] * 5 + [vmem] * 2 + [smem] * 2 + [vmem] * 4 + [smem] * 2,
+        in_specs=[hbm] * 15,
         out_specs=(vmem,) * 3,
         scratch_shapes=[
+            pltpu.VMEM(bw.shape, bf16),
+            pltpu.VMEM(dw.shape, bf16),
+            pltpu.SMEM(bias.shape, f32),
+            pltpu.SMEM(rate.shape, f32),
+            pltpu.VMEM(gain.shape, f32),
+            pltpu.VMEM(nq.shape, bf16),
+            pltpu.VMEM(nk.shape, bf16),
+            pltpu.VMEM(nv.shape, bf16),
+            pltpu.SMEM(nb.shape, f32),
+            pltpu.SMEM(nd.shape, f32),
+            dma((10,)),
             pltpu.VMEM((2 * PAD, bw.shape[1]), bf16),
             pltpu.VMEM((tn, seqs, span, kd), bf16),
             pltpu.VMEM((4, tn, kd, width), bf16),
             pltpu.VMEM((seqs, 4, span, width), f32),
             pltpu.VMEM((seqs, 2 * PAD, span), f32),
-            pltpu.VMEM((3, span, span), bf16),
+            pltpu.VMEM((seqs, PAD, span), f32),
             pltpu.VMEM((seqs, span, PAD), f32),
             pltpu.VMEM((heads, span, extent), bf16),
-            pltpu.VMEM((heads, span, span), f32),
             pltpu.VMEM((heads, span, 2 * extent), bf16),
             pltpu.VMEM((seqs, heads, span, extent), f32),
             pltpu.VMEM((seqs, heads, span, extent), bf16),
@@ -575,8 +627,10 @@
             pltpu.VMEM((seqs, extent, extent), bf16),
             pltpu.VMEM((seqs, g, extent, extent), bf16),
             pltpu.VMEM((seqs, heads, extent, extent), bf16),
-            pltpu.VMEM((seqs, sn, tail, extent), f32),
-            pltpu.VMEM((seqs, heads, tail, extent), f32),
+            pltpu.VMEM((seqs, sn, key_rows, extent), bf16),
+            pltpu.VMEM((seqs, heads, key_rows, extent), bf16),
+            pltpu.VMEM((seqs, 1, extent), f32),
+            pltpu.VMEM((seqs, heads, 1, extent), f32),
             dma((seqs,)),
             dma((4, tn)),
             dma((chips - 1, seqs, chunks)),
@@ -590,6 +644,8 @@
             dma((seqs, heads)),
             dma((seqs,)),
             dma((seqs,)),
+            dma((seqs, sn)),
+            dma((seqs, heads)),
             dma((seqs, sn)),
             dma((seqs, heads)),
             pltpu.SemaphoreType.REGULAR,

time: 46.1 us -> 43.5 us (0.944)
  Pallas kernels: 45.2 us -> 42.7 us
    pallas_call x1, Pallas kernels: 44.4 us -> 41.9 us  [fused(): pl.pallas_call(functools.partial(fused_kernel, tn, sn, seqs, heads), out_...]
where the time goes in v3:
time: 43.5 us; the launch traced here: 43.3 us
  Pallas kernels  42.7 us (98%)
  between operations  0.64 us (1%)
    pallas_call x1, Pallas kernels, fused(): pl.pallas_call(functools.partial(fused_kernel, tn, sn, seqs, heads), out_...  41.9 us

profile of v3, /device:TPU:0, one launch (start us, length us, event | category | flops | bytes accessed | tf_op | source)
XLA Modules:
  0.0 43.3 jit_solution(12222622955258789338)
XLA Ops:
  0.6 41.9 %shard_map.166 = (bf16[384,512]{1,0:T(8,128)(2,1)S(1)}, bf16[8,16,128]{2,1,0:T(8,128)(2,1)S(1)}, f32[2,512]{1,0:T(2,128)S(1)}) custom-call(bf16[384,1024]{1,0:T(8,128)(2,1)} %bitcast.8, bf16[4096,512]{1,0:T(8,128)(2,1)} %wq_ref.1, bf16[4096,512]{1,0:T(8,128)(2,1)} %wk_ref.1, bf16[4096,512]{1,0:T(8,128)(2,1)} %wv_ref.1, bf16[4096,512]{1,0:T(8,128)(2,1)} %wg_ref.1, ...), custom_call_target="tpu_custom_call" | custom-call | tf_op jit(solution)/shard_map/pallas_call | solution.py:591
  42.5 0.8 %shard_map.167 = (bf16[2,192,512]{2,1,0:T(8,128)(2,1)}, bf16[2,4,16,128]{3,2,1,0:T(8,128)(2,1)}, f32[2,512]{1,0:T(2,128)}) custom-call(bf16[2,192,512]{2,1,0:T(8,128)(2,1)S(1)} %bitcast.6, bf16[2,4,16,128]{3,2,1,0:T(8,128)(2,1)S(1)} %bitcast.7, f32[2,512]{1,0:T(2,128)S(1)} %get-tuple-element.8.first_ref), custom_call_target="tpu_custom_call" | custom-call | tf_op jit(solution)/shard_map/pallas_call | solution.py:671

commit v4 on v3

--- a/solution.py
+++ b/solution.py
@@ -41,7 +41,7 @@
     nq_hbm, nk_hbm, nv_hbm, nb_hbm, nd_hbm, mixed_ref, cache_ref, first_ref,
     bw_ref, dw_ref, bias_ref, rate_ref, gain_ref, nq_ref, nk_ref, nv_ref, nb_ref, nd_ref, small_sem,
     bd, xs, wbuf, acc, sacc, cum_row, cum_col, kh_buf, uw_buf, local_out, reach, gated,
-    out_box, in_box, mid_out, mid_in, back_out, back_in, tail_out, tail_in, word_out, word_in,
+    out_box, in_box, mid_out, mid_in, back_out, back_in, tail_out, tail_in, word_out, word_in, moves, drives, asks, extra,
     xsem, wsem, cross_sem, part_sem, fwd_sem, rx, prx,
     send1, recv1, send2, recv2, send3, recv3, send4, recv4, send5, recv5, hello,
 ):
@@ -49,7 +49,7 @@
     width = wq_ref.shape[1]
     extent = width // heads
     key_rows = extent // sn
-    chunks = rx.shape[2]
+    chunks = rx.shape[3]
     kc = kd // chunks
     tme, me = lax.axis_index("tp"), lax.axis_index("sp")
     y, c = tme // 2, lax.rem(tme, 2)
@@ -85,7 +85,7 @@
     def weight_copy(w, slot):
         start = pl.multiple_of(order[slot] * kd, kd)
         return pltpu.make_async_copy(
-            weights[w].at[pl.ds(start, kd), :], wbuf.at[w, slot], wsem.at[w, slot]
+            weights[w].at[pl.ds(start, kd), :], wbuf.at[slot, w], wsem.at[slot]
         )
 
     small_copies = [
@@ -107,14 +107,14 @@
         to = lax.rem(y + d, chips) * 2 + c
         return pltpu.make_async_remote_copy(
             src_ref=xs.at[tme, s, :, cols(ck)], dst_ref=xs.at[tme, s, :, cols(ck)],
-            send_sem=cross_sem.at[d - 1, s, ck], recv_sem=rx.at[tme, s, ck],
+            send_sem=cross_sem.at[d - 1], recv_sem=rx.at[d - 1, 0, s, ck],
             device_id={"tp": to}, device_id_type=MESH,
         )
 
     def part_copy(s):
         return pltpu.make_async_remote_copy(
             src_ref=xs.at[tme, s], dst_ref=xs.at[tme, s],
-            send_sem=part_sem.at[s], recv_sem=prx.at[s],
+            send_sem=part_sem.at[0], recv_sem=prx.at[s],
             device_id={"tp": partner}, device_id_type=MESH,
         )
 
@@ -151,14 +151,15 @@
         b = order[2 * d]
         return pltpu.make_async_remote_copy(
             src_ref=xs.at[b, s, :, cols(ck)], dst_ref=xs.at[b, s, :, cols(ck)],
-            send_sem=fwd_sem.at[d - 1, s, ck], recv_sem=rx.at[b, s, ck],
+            send_sem=fwd_sem.at[d - 1], recv_sem=rx.at[d - 1, 1, s, ck],
             device_id={"tp": partner}, device_id_type=MESH,
         )
 
-    def arrive(b, s, ck):
+    def arrive(d, side, s, ck):
+        b = order[2 * d + side]
         pltpu.make_async_remote_copy(
             src_ref=xs.at[b, s, :, cols(ck)], dst_ref=xs.at[b, s, :, cols(ck)],
-            send_sem=part_sem.at[0], recv_sem=rx.at[b, s, ck],
+            send_sem=part_sem.at[0], recv_sem=rx.at[d - 1, side, s, ck],
             device_id={"tp": partner}, device_id_type=MESH,
         ).wait_recv()
 
@@ -170,30 +171,34 @@
     def use_whole(slot, s):
         b = order[slot]
         x = xs[b, s]
+        if s == 0:
+            weights_wait(slot)
         for w in range(4):
-            if s == 0:
-                weight_copy(w, slot).wait()
-            term = dot(x, wbuf[w, slot])
+            term = dot(x, wbuf[slot, w])
             acc[s, w] = term if slot == 0 else acc[s, w] + term
         small(x, b * kd, kd, s, slot == 0)
 
-    def use(slot, s, ck):
+    def weights_wait(slot):
+        pltpu.make_async_copy(wbuf.at[slot], wbuf.at[slot], wsem.at[slot]).wait()
+
+    def use(slot, s, ck, parts=(1, 2, 0, 3)):
         b = order[slot]
         x = xs[b, s, :, cols(ck)]
-        for w in range(4):
+        if 1 in parts:
             if s == 0 and ck == 0:
-                weight_copy(w, slot).wait()
-            acc[s, w] += dot(x, wbuf[w, slot, cols(ck), :])
-        small(x, b * kd + ck * kc, kc, s, False)
+                weights_wait(slot)
+            small(x, b * kd + ck * kc, kc, s, False)
+        for w in parts:
+            acc[s, w] += dot(x, wbuf[slot, w, cols(ck), :])
 
     def forward(d, s, ck):
-        arrive(order[2 * d], s, ck)
+        arrive(d, 0, s, ck)
         fwd_copy(d, s, ck).start()
 
-    def finish_chunk(d, s, ck):
-        use(2 * d, s, ck)
-        arrive(order[2 * d + 1], s, ck)
-        use(2 * d + 1, s, ck)
+    def finish_chunk(d, s, ck, parts):
+        use(2 * d, s, ck, parts)
+        arrive(d, 1, s, ck)
+        use(2 * d + 1, s, ck, parts)
 
     def heads_of(w, s):
         return [acc[s, w, :, h * extent : (h + 1) * extent].astype(bf16).astype(f32) for h in range(heads)]
@@ -204,7 +209,7 @@
     def box_copy(s, h):
         return pltpu.make_async_remote_copy(
             src_ref=out_box.at[s, h], dst_ref=in_box.at[s, m],
-            send_sem=send1.at[s, h], recv_sem=recv1.at[s, m],
+            send_sem=send1.at[s], recv_sem=recv1.at[s],
             device_id={"sp": team * g + owner_of(s, h)}, device_id_type=MESH,
         )
 
@@ -212,8 +217,13 @@
         beta = jax.nn.sigmoid(sacc[s, 0:PAD, :] + bias)
         pre = sacc[s, PAD : 2 * PAD, :]
         soft = jnp.maximum(pre, 0.0) + jnp.log1p(jnp.exp(-jnp.abs(pre)))
-        upper = jnp.where(row <= col, 1.0, 0.0)
-        cum = dot(-jnp.exp(rate) * soft, upper, NN, highest)
+        upper = jnp.where(row <= col, 1.0, 0.0).astype(bf16)
+        rest, pieces = -jnp.exp(rate) * soft, []
+        for _ in range(3):
+            pieces.append(rest.astype(bf16).astype(f32))
+            rest = rest - pieces[-1]
+        sums = dot(jnp.concatenate(pieces, axis=0).astype(bf16), upper)
+        cum = sums[0:PAD] + sums[PAD : 2 * PAD] + sums[2 * PAD :]
         cum_t, beta_t = cum.T, beta.T
         cum_row[s] = cum
         cum_col[s] = cum_t
@@ -333,7 +343,7 @@
     def back_copy(s, i):
         return pltpu.make_async_remote_copy(
             src_ref=back_out.at[s, i], dst_ref=back_in.at[s, own_head(s)],
-            send_sem=send2.at[s, i], recv_sem=recv2.at[s, own_head(s)],
+            send_sem=send2.at[s], recv_sem=recv2.at[s],
             device_id={"sp": team * g + i}, device_id_type=MESH,
         )
 
@@ -347,23 +357,20 @@
         h = own_head(s)
         return (
             pltpu.make_async_remote_copy(
-                src_ref=tail_out.at[s, j], dst_ref=tail_in.at[s, h], send_sem=send4.at[s, j], recv_sem=recv4.at[s, h],
+                src_ref=tail_out.at[s, j], dst_ref=tail_in.at[s, h], send_sem=send4.at[s], recv_sem=recv4.at[s],
                 device_id={"sp": j}, device_id_type=MESH,
             ),
             pltpu.make_async_remote_copy(
-                src_ref=word_out.at[s], dst_ref=word_in.at[s, h], send_sem=send5.at[s, j], recv_sem=recv5.at[s, h],
+                src_ref=word_out.at[s, j], dst_ref=word_in.at[s, h], send_sem=send5.at[s], recv_sem=recv5.at[s],
                 device_id={"sp": j}, device_id_type=MESH,
             ),
         )
 
-    def box_wait(s, i):
-        @pl.when(i != m)
-        def _():
-            pltpu.make_async_remote_copy(
-                src_ref=out_box.at[s, 0], dst_ref=in_box.at[s, i],
-                send_sem=send1.at[s, 0], recv_sem=recv1.at[s, i],
-                device_id={"sp": team * g + i}, device_id_type=MESH,
-            ).wait_recv()
+    def settle(ref, sem):
+        pltpu.make_async_copy(ref, ref, sem).wait()
+
+    def box_wait(s):
+        settle(in_box.at[s, pl.ds(0, g - 1)], recv1.at[s])
 
     def give_back(s):
         for i in range(g):
@@ -376,35 +383,45 @@
             def _():
                 back_copy(s, i).start()
 
+    def prepare(s):
+        h = own_head(s)
+        shape3 = nq_ref.shape
+        mine = (lax.broadcasted_iota(jnp.int32, shape3, 0) == s) & (lax.broadcasted_iota(jnp.int32, shape3, 1) == h)
+
+        def own(ref):
+            kept = jnp.where(mine, ref[...].astype(f32), 0.0)
+            return jnp.sum(jnp.sum(kept, axis=0), axis=0, keepdims=True)
+
+        qn, kn = unit_rows(own(nq_ref)), unit_rows(own(nk_ref))
+        rest = jnp.concatenate([jnp.broadcast_to(qn, (PAD, extent)), jnp.broadcast_to(kn, (PAD, extent))], axis=0)
+        for i in range(3):
+            piece = rest.astype(bf16)
+            asks[s, i * 2 * PAD : (i + 1) * 2 * PAD] = piece
+            rest = rest - piece.astype(f32)
+        extra[s, 0:1] = own(nv_ref)
+        extra[s, 1:2] = jnp.broadcast_to(jnp.sum(kn * qn, axis=-1, keepdims=True), (1, extent))
+
     def conclude(s, final):
         kept_h = final.astype(bf16)
-        memory = kept_h.astype(f32)
         h = own_head(s)
         for j in range(sn):
             tail_out[s, j] = kept_h[j * key_rows : (j + 1) * key_rows]
-        shape3 = nq_ref.shape
-        mine = (lax.broadcasted_iota(jnp.int32, shape3, 0) == s) & (lax.broadcasted_iota(jnp.int32, shape3, 1) == h)
-
-        def own(ref):
-            kept = jnp.where(mine, ref[...].astype(f32), 0.0)
-            return jnp.sum(jnp.sum(kept, axis=0), axis=0, keepdims=True)
-
-        qn, kn = unit_rows(own(nq_ref)), unit_rows(own(nk_ref))
-        both = jnp.concatenate([jnp.broadcast_to(qn, (PAD, extent)), jnp.broadcast_to(kn, (PAD, extent))], axis=0)
-        reads = dot(both, memory, NN, highest)
-        recall, retrieve = reads[0:1], reads[PAD : PAD + 1]
+        sums = dot(asks[s], kept_h)
+        sums = sums[0 : 2 * PAD] + sums[2 * PAD : 4 * PAD] + sums[4 * PAD :]
+        recall, retrieve = sums[0:1], sums[PAD : PAD + 1]
         beta_new, decay_new = nb_ref[s, h], nd_ref[s, h]
-        fresh = own(nv_ref) - decay_new * retrieve
-        meet = jnp.sum(kn * qn, axis=-1, keepdims=True)
-        read = decay_new * recall + (beta_new * meet) * fresh
+        fresh = extra[s, 0:1] - decay_new * retrieve
+        read = decay_new * recall + (beta_new * extra[s, 1:2]) * fresh
         norm = lax.rsqrt(jnp.mean(read * read, axis=-1, keepdims=True) + norm_floor)
-        word_out[s] = read * norm * gain_ref[...]
+        word = read * norm * gain_ref[...]
         for j in range(sn):
+            word_out[s, j] = word
+        for j in range(sn):
 
             @pl.when(j == me)
             def _():
                 tail_in[s, h] = tail_out[s, j]
-                word_in[s, h] = word_out[s]
+                word_in[s, h] = word_out[s, j]
 
             @pl.when(j != me)
             def _():
@@ -414,8 +431,9 @@
     def chain_first(s):
         @pl.when((own_head(s) < heads) & (team == 0))
         def _():
-            for i in range(g):
-                box_wait(s, i)
+            if groups == 1:
+                prepare(s)
+            box_wait(s)
             state = jnp.zeros((extent, extent), f32)
             for i in range(g):
                 half = state.astype(bf16)
@@ -431,59 +449,69 @@
                 conclude(s, state)
             give_back(s)
 
-    def chain_later(s):
+    def compose(s):
         if groups == 1:
             return
 
         @pl.when((own_head(s) < heads) & (team > 0))
         def _():
-            for i in range(g):
-                box_wait(s, i)
-            shift, drive = [None], [None]
+            prepare(s)
+            box_wait(s)
             for i in range(g):
                 step, push = in_box[s, i, 0], in_box[s, i, 1].astype(f32)
                 if i == 0:
-                    shift.append(step.astype(f32))
-                    drive.append(push)
+                    shift, drive = step.astype(f32), push
                 else:
-                    shift.append(shift[i] + step.astype(f32) + dot(step, shift[i].astype(bf16)))
-                    drive.append(drive[i] + push + dot(step, drive[i].astype(bf16)))
-            moves = jnp.concatenate([a.astype(bf16) for a in shift[1:]], axis=0)
+                    shift, drive = (
+                        shift + step.astype(f32) + dot(step, shift.astype(bf16)),
+                        drive + push + dot(step, drive.astype(bf16)),
+                    )
+                moves[s, i * extent : (i + 1) * extent] = shift.astype(bf16)
+                drives[s, i * extent : (i + 1) * extent] = drive
+
+    def relay(s):
+        if groups == 1:
+            return
+
+        @pl.when((own_head(s) < heads) & (team > 0))
+        def _():
             pltpu.make_async_remote_copy(
                 src_ref=mid_out.at[s], dst_ref=mid_in.at[s], send_sem=send3.at[s], recv_sem=recv3.at[s],
                 device_id={"sp": lax.rem(me + sn - g, sn)}, device_id_type=MESH,
             ).wait_recv()
             start = mid_in[s]
-            moved = dot(moves, start)
             base = start.astype(f32)
+            top = (g - 1) * extent
+            state = base + dot(moves[s, top:], start) + drives[s, top:]
+
+            @pl.when(team < groups - 1)
+            def _():
+                mid_out[s] = state.astype(bf16)
+                mid_copy(s).start()
+
+            @pl.when(team == groups - 1)
+            def _():
+                conclude(s, state)
+
+            moved = dot(moves[s, :top], start) + drives[s, :top]
             back_out[s, 0] = start
             for i in range(1, g):
-                back_out[s, i] = (base + moved[(i - 1) * extent : i * extent] + drive[i]).astype(bf16)
-            state = base + moved[(g - 1) * extent :] + drive[g]
-
-            @pl.when(team < groups - 1)
-            def _():
-                mid_out[s] = state.astype(bf16)
-                mid_copy(s).start()
-
-            @pl.when(team == groups - 1)
-            def _():
-                conclude(s, state)
-
+                back_out[s, i] = (base + moved[(i - 1) * extent : i * extent]).astype(bf16)
             give_back(s)
 
+    def arrivals(owner, ref, sem):
+        if heads > 1:
+
+            @pl.when(owner)
+            def _():
+                settle(ref.at[pl.ds(0, heads - 1)], sem)
+
+        @pl.when(jnp.logical_not(owner))
+        def _():
+            settle(ref, sem)
+
     def finish(s):
-        for h in range(heads):
-            o = owner_of(s, h)
-
-            @pl.when(m != o)
-            def _():
-                pltpu.make_async_remote_copy(
-                    src_ref=back_out.at[s, 0], dst_ref=back_in.at[s, h],
-                    send_sem=send2.at[s, 0], recv_sem=recv2.at[s, h],
-                    device_id={"sp": team * g + o}, device_id_type=MESH,
-                ).wait_recv()
-
+        arrivals(own_head(s) < heads, back_in.at[s], recv2.at[s])
         outs = [local_out[s, h] + dot(reach[s, h], back_in[s, h]) for h in range(heads)]
         for h in range(heads):
             o = outs[h]
@@ -491,22 +519,10 @@
             mixed_ref[s * span : (s + 1) * span, h * extent : (h + 1) * extent] = (o * norm * gated[s, h]).astype(bf16)
 
     def take_tail(s):
+        source = (team == groups - 1) & (own_head(s) < heads)
+        arrivals(source, tail_in.at[s], recv4.at[s])
+        arrivals(source, word_in.at[s], recv5.at[s])
         for h in range(heads):
-            source = (groups - 1) * g + owner_of(s, h)
-
-            @pl.when(me != source)
-            def _():
-                pltpu.make_async_remote_copy(
-                    src_ref=tail_out.at[s, 0], dst_ref=tail_in.at[s, h],
-                    send_sem=send4.at[s, 0], recv_sem=recv4.at[s, h],
-                    device_id={"sp": source}, device_id_type=MESH,
-                ).wait_recv()
-                pltpu.make_async_remote_copy(
-                    src_ref=word_out.at[s], dst_ref=word_in.at[s, h],
-                    send_sem=send5.at[s, 0], recv_sem=recv5.at[s, h],
-                    device_id={"sp": source}, device_id_type=MESH,
-                ).wait_recv()
-
             cache_ref[s * heads + h] = tail_in[s, h]
             first_ref[s : s + 1, h * extent : (h + 1) * extent] = word_in[s, h]
 
@@ -514,7 +530,7 @@
         use_whole(0, s)
     for s in range(seqs):
         pltpu.make_async_remote_copy(
-            src_ref=xs.at[partner, s], dst_ref=xs.at[partner, s], send_sem=part_sem.at[s], recv_sem=prx.at[s],
+            src_ref=xs.at[partner, s], dst_ref=xs.at[partner, s], send_sem=part_sem.at[0], recv_sem=prx.at[s],
             device_id={"tp": partner}, device_id_type=MESH,
         ).wait_recv()
         use_whole(1, s)
@@ -524,40 +540,35 @@
             for d in range(1, chips):
                 if s == 0 or ck > 0:
                     forward(d, s, ck)
-                if s > 0 and ck == chunks - 1 and d == chips - 1:
-                    chain_first(s - 1)
-                finish_chunk(d, s, ck)
+                finish_chunk(d, s, ck, (1, 2) if ck == chunks - 1 else (1, 2, 0, 3))
         boxes(s)
         if s > 0:
-            chain_later(s - 1)
+            chain_first(s - 1)
+            compose(s - 1)
         if s < seqs - 1:
             for d in range(1, chips):
                 forward(d, s + 1, 0)
+        for slot in range(2, tn):
+            use(slot, s, chunks - 1, (0, 3))
         queries(s)
-    for s in range(seqs - 1):
+        if s > 0:
+            relay(s - 1)
+    compose(seqs - 1)
+    chain_first(seqs - 1)
+    relay(seqs - 1)
+    for s in range(seqs):
         finish(s)
-    chain_first(seqs - 1)
-    chain_later(seqs - 1)
-    finish(seqs - 1)
+    settle(xs.at[tme], part_sem.at[0])
+    for d in range(1, chips):
+        settle(xs.at[tme], cross_sem.at[d - 1])
+        settle(xs.at[tme], fwd_sem.at[d - 1])
     for s in range(seqs):
-        part_copy(s).wait_send()
-        for ck in range(chunks):
-            for d in range(1, chips):
-                cross_copy(d, s, ck).wait_send()
-                fwd_copy(d, s, ck).wait_send()
-        for h in range(heads):
-
-            @pl.when(m != owner_of(s, h))
-            def _():
-                box_copy(s, h).wait_send()
-
-        @pl.when(own_head(s) < heads)
+        own = own_head(s) < heads
+        arrivals(own, out_box.at[s], send1.at[s])
+
+        @pl.when(own)
         def _():
-            for i in range(g):
-
-                @pl.when(i != m)
-                def _():
-                    back_copy(s, i).wait_send()
+            settle(back_out.at[s, pl.ds(0, g - 1)], send2.at[s])
 
             @pl.when(team < groups - 1)
             def _():
@@ -565,12 +576,8 @@
 
             @pl.when(team == groups - 1)
             def _():
-                for j in range(sn):
-
-                    @pl.when(j != me)
-                    def _():
-                        for copy in tail_copies(s, j):
-                            copy.wait_send()
+                settle(tail_out.at[s, pl.ds(0, sn - 1)], send4.at[s])
+                settle(word_out.at[s, pl.ds(0, sn - 1)], send5.at[s])
 
     for s in range(seqs):
         take_tail(s)
@@ -611,7 +618,7 @@
             dma((10,)),
             pltpu.VMEM((2 * PAD, bw.shape[1]), bf16),
             pltpu.VMEM((tn, seqs, span, kd), bf16),
-            pltpu.VMEM((4, tn, kd, width), bf16),
+            pltpu.VMEM((tn, 4, kd, width), bf16),
             pltpu.VMEM((seqs, 4, span, width), f32),
             pltpu.VMEM((seqs, 2 * PAD, span), f32),
             pltpu.VMEM((seqs, PAD, span), f32),
@@ -629,25 +636,29 @@
             pltpu.VMEM((seqs, heads, extent, extent), bf16),
             pltpu.VMEM((seqs, sn, key_rows, extent), bf16),
             pltpu.VMEM((seqs, heads, key_rows, extent), bf16),
-            pltpu.VMEM((seqs, 1, extent), f32),
+            pltpu.VMEM((seqs, sn, 1, extent), f32),
             pltpu.VMEM((seqs, heads, 1, extent), f32),
-            dma((seqs,)),
-            dma((4, tn)),
-            dma((chips - 1, seqs, chunks)),
-            dma((seqs,)),
-            dma((chips - 1, seqs, chunks)),
-            dma((tn, seqs, chunks)),
-            dma((seqs,)),
-            dma((seqs, heads)),
-            dma((seqs, g)),
-            dma((seqs, g)),
-            dma((seqs, heads)),
-            dma((seqs,)),
-            dma((seqs,)),
-            dma((seqs, sn)),
-            dma((seqs, heads)),
-            dma((seqs, sn)),
-            dma((seqs, heads)),
+            pltpu.VMEM((seqs, g * extent, extent), bf16),
+            pltpu.VMEM((seqs, g * extent, extent), f32),
+            pltpu.VMEM((seqs, 6 * PAD, extent), bf16),
+            pltpu.VMEM((seqs, PAD, extent), f32),
+            dma((seqs,)),
+            dma((tn,)),
+            dma((chips - 1,)),
+            dma((1,)),
+            dma((chips - 1,)),
+            dma((chips - 1, 2, seqs, chunks)),
+            dma((seqs,)),
+            dma((seqs,)),
+            dma((seqs,)),
+            dma((seqs,)),
+            dma((seqs,)),
+            dma((seqs,)),
+            dma((seqs,)),
+            dma((seqs,)),
+            dma((seqs,)),
+            dma((seqs,)),
+            dma((seqs,)),
             pltpu.SemaphoreType.REGULAR,
         ],
         compiler_params=pltpu.CompilerParams(

time: 43.5 us -> 41.8 us (0.961)
  Pallas kernels: 42.7 us -> 41 us
    pallas_call x1, Pallas kernels: 41.9 us -> 40.3 us  [fused(): pl.pallas_call(functools.partial(fused_kernel, tn, sn, seqs, heads), out_...]
where the time goes in v4:
time: 41.8 us; the launch traced here: 41.7 us
  Pallas kernels  41 us (98%)
  between operations  0.64 us (2%)
    pallas_call x1, Pallas kernels, fused(): pl.pallas_call(functools.partial(fused_kernel, tn, sn, seqs, heads), out_...  40.3 us

profile of v4, /device:TPU:0, one launch (start us, length us, event | category | flops | bytes accessed | tf_op | source)
XLA Modules:
  0.0 41.7 jit_solution(9251509363676794940)
XLA Ops:
  0.6 40.3 %shard_map.166 = (bf16[384,512]{1,0:T(8,128)(2,1)S(1)}, bf16[8,16,128]{2,1,0:T(8,128)(2,1)S(1)}, f32[2,512]{1,0:T(2,128)S(1)}) custom-call(bf16[384,1024]{1,0:T(8,128)(2,1)} %bitcast.8, bf16[4096,512]{1,0:T(8,128)(2,1)} %wq_ref.1, bf16[4096,512]{1,0:T(8,128)(2,1)} %wk_ref.1, bf16[4096,512]{1,0:T(8,128)(2,1)} %wv_ref.1, bf16[4096,512]{1,0:T(8,128)(2,1)} %wg_ref.1, ...), custom_call_target="tpu_custom_call" | custom-call | tf_op jit(solution)/shard_map/pallas_call | solution.py:598
  40.9 0.8 %shard_map.167 = (bf16[2,192,512]{2,1,0:T(8,128)(2,1)}, bf16[2,4,16,128]{3,2,1,0:T(8,128)(2,1)}, f32[2,512]{1,0:T(2,128)}) custom-call(bf16[2,192,512]{2,1,0:T(8,128)(2,1)S(1)} %bitcast.6, bf16[2,4,16,128]{3,2,1,0:T(8,128)(2,1)S(1)} %bitcast.7, f32[2,512]{1,0:T(2,128)S(1)} %get-tuple-element.8.first_ref), custom_call_target="tpu_custom_call" | custom-call | tf_op jit(solution)/shard_map/pallas_call | solution.py:682

commit v5 on v4

--- a/solution.py
+++ b/solution.py
@@ -41,9 +41,9 @@
     nq_hbm, nk_hbm, nv_hbm, nb_hbm, nd_hbm, mixed_ref, cache_ref, first_ref,
     bw_ref, dw_ref, bias_ref, rate_ref, gain_ref, nq_ref, nk_ref, nv_ref, nb_ref, nd_ref, small_sem,
     bd, xs, wbuf, acc, sacc, cum_row, cum_col, kh_buf, uw_buf, local_out, reach, gated,
-    out_box, in_box, mid_out, mid_in, back_out, back_in, tail_out, tail_in, word_out, word_in, moves, drives, asks, extra,
+    out_box, in_box, mid_out, mid_in, back_out, back_in, tail_out, tail_in, moves, drives, asks, extra, news, news_sem,
     xsem, wsem, cross_sem, part_sem, fwd_sem, rx, prx,
-    send1, recv1, send2, recv2, send3, recv3, send4, recv4, send5, recv5, hello,
+    send1, recv1, send2, recv2, send3, recv3, send4, recv4, hello,
 ):
     _, _, span, kd = xs.shape
     width = wq_ref.shape[1]
@@ -69,7 +69,8 @@
 
         @pl.when(me + d < sn)
         def _():
-            pl.semaphore_signal(barrier, inc=1, device_id={"sp": me + d}, device_id_type=MESH)
+            for t in (tme, partner):
+                pl.semaphore_signal(barrier, inc=1, device_id={"sp": me + d, "tp": t}, device_id_type=MESH)
 
     order = [tme, partner]
     for d in range(1, chips):
@@ -101,7 +102,7 @@
         token_copy(s).start()
     for copy in small_copies:
         copy.start()
-    pl.semaphore_wait(barrier, chips + me)
+    pl.semaphore_wait(barrier, chips + 2 * me)
 
     def cross_copy(d, s, ck):
         to = lax.rem(y + d, chips) * 2 + c
@@ -131,10 +132,28 @@
 
         @pl.when(me >= d)
         def _():
-            pl.semaphore_signal(hello, inc=1, device_id={"sp": me - d}, device_id_type=MESH)
+            for t in (tme, partner):
+                pl.semaphore_signal(hello, inc=1, device_id={"sp": me - d, "tp": t}, device_id_type=MESH)
 
     for copy in small_copies:
         copy.wait()
+    for s in range(seqs):
+        for i, ref in enumerate((nq_ref, nk_ref, nv_ref)):
+            news[c, i, s * heads : (s + 1) * heads] = ref[s].astype(f32)
+        for i, ref in enumerate((nb_ref, nd_ref)):
+            for h in range(heads):
+                news[c, 3 + i, s * heads + h : s * heads + h + 1] = jnp.full((1, extent), ref[s, h], f32)
+
+    def news_copy():
+        return pltpu.make_async_remote_copy(
+            src_ref=news.at[0], dst_ref=news.at[0], send_sem=news_sem.at[0], recv_sem=news_sem.at[1],
+            device_id={"tp": partner}, device_id_type=MESH,
+        )
+
+    @pl.when(c == 0)
+    def _():
+        news_copy().start()
+
     bd[...] = jnp.zeros_like(bd)
     bd[0 : bw_ref.shape[0]] = bw_ref[...]
     bd[PAD : PAD + dw_ref.shape[0]] = dw_ref[...]
@@ -208,9 +227,9 @@
 
     def box_copy(s, h):
         return pltpu.make_async_remote_copy(
-            src_ref=out_box.at[s, h], dst_ref=in_box.at[s, m],
+            src_ref=out_box.at[s, h], dst_ref=in_box.at[s, (1 - c) * g + m],
             send_sem=send1.at[s], recv_sem=recv1.at[s],
-            device_id={"sp": team * g + owner_of(s, h)}, device_id_type=MESH,
+            device_id={"sp": team * g + owner_of(s, h), "tp": y * 2 + 1}, device_id_type=MESH,
         )
 
     def boxes(s):
@@ -305,10 +324,10 @@
 
             @pl.when(me < sn - 1)
             def _():
-                pl.semaphore_wait(hello, sn - 1 - me)
+                pl.semaphore_wait(hello, 2 * (sn - 1 - me))
 
         for h in hs:
-            own = m == owner_of(s, h)
+            own = (m == owner_of(s, h)) & (c == 1)
 
             @pl.when(own)
             def _():
@@ -340,11 +359,14 @@
     def own_head(s):
         return lax.rem(m + g - (s * heads) % g, g)
 
-    def back_copy(s, i):
+    def owner(s):
+        return (own_head(s) < heads) & (c == 1)
+
+    def back_copy(s, e, i):
         return pltpu.make_async_remote_copy(
-            src_ref=back_out.at[s, i], dst_ref=back_in.at[s, own_head(s)],
+            src_ref=back_out.at[s, e * g + i], dst_ref=back_in.at[s, own_head(s)],
             send_sem=send2.at[s], recv_sem=recv2.at[s],
-            device_id={"sp": team * g + i}, device_id_type=MESH,
+            device_id={"sp": team * g + i, "tp": y * 2 + 1 - e}, device_id_type=MESH,
         )
 
     def mid_copy(s):
@@ -353,27 +375,22 @@
             device_id={"sp": lax.rem(me + g, sn)}, device_id_type=MESH,
         )
 
-    def tail_copies(s, j):
-        h = own_head(s)
-        return (
-            pltpu.make_async_remote_copy(
-                src_ref=tail_out.at[s, j], dst_ref=tail_in.at[s, h], send_sem=send4.at[s], recv_sem=recv4.at[s],
-                device_id={"sp": j}, device_id_type=MESH,
-            ),
-            pltpu.make_async_remote_copy(
-                src_ref=word_out.at[s, j], dst_ref=word_in.at[s, h], send_sem=send5.at[s], recv_sem=recv5.at[s],
-                device_id={"sp": j}, device_id_type=MESH,
-            ),
+    def tail_copy(s, e, j):
+        return pltpu.make_async_remote_copy(
+            src_ref=tail_out.at[s, e * sn + j], dst_ref=tail_in.at[s, own_head(s)],
+            send_sem=send4.at[s], recv_sem=recv4.at[s],
+            device_id={"sp": j, "tp": y * 2 + 1 - e}, device_id_type=MESH,
         )
 
     def settle(ref, sem):
         pltpu.make_async_copy(ref, ref, sem).wait()
 
     def box_wait(s):
-        settle(in_box.at[s, pl.ds(0, g - 1)], recv1.at[s])
+        settle(in_box.at[s, pl.ds(0, 2 * g - 1)], recv1.at[s])
 
     def give_back(s):
         for i in range(g):
+            back_copy(s, 1, i).start()
 
             @pl.when(i == m)
             def _():
@@ -381,69 +398,74 @@
 
             @pl.when(i != m)
             def _():
-                back_copy(s, i).start()
+                back_copy(s, 0, i).start()
 
     def prepare(s):
-        h = own_head(s)
-        shape3 = nq_ref.shape
-        mine = (lax.broadcasted_iota(jnp.int32, shape3, 0) == s) & (lax.broadcasted_iota(jnp.int32, shape3, 1) == h)
-
-        def own(ref):
-            kept = jnp.where(mine, ref[...].astype(f32), 0.0)
-            return jnp.sum(jnp.sum(kept, axis=0), axis=0, keepdims=True)
-
-        qn, kn = unit_rows(own(nq_ref)), unit_rows(own(nk_ref))
-        rest = jnp.concatenate([jnp.broadcast_to(qn, (PAD, extent)), jnp.broadcast_to(kn, (PAD, extent))], axis=0)
-        for i in range(3):
-            piece = rest.astype(bf16)
-            asks[s, i * 2 * PAD : (i + 1) * 2 * PAD] = piece
-            rest = rest - piece.astype(f32)
-        extra[s, 0:1] = own(nv_ref)
-        extra[s, 1:2] = jnp.broadcast_to(jnp.sum(kn * qn, axis=-1, keepdims=True), (1, extent))
-
-    def conclude(s, final):
-        kept_h = final.astype(bf16)
-        h = own_head(s)
+        r = s * heads + own_head(s)
+        for e in range(2):
+            told = [news[1 - e, i, pl.ds(r, 1), :] for i in range(3)]
+            qn, kn = unit_rows(told[0]), unit_rows(told[1])
+            rest = jnp.concatenate([jnp.broadcast_to(qn, (PAD, extent)), jnp.broadcast_to(kn, (PAD, extent))], axis=0)
+            for i in range(3):
+                piece = rest.astype(bf16)
+                asks[s, e, i * 2 * PAD : (i + 1) * 2 * PAD] = piece
+                rest = rest - piece.astype(f32)
+            decay, meet = news[1 - e, 4, pl.ds(r, 1), :], jnp.sum(kn * qn, axis=-1, keepdims=True)
+            extra[s, e, 0:1] = told[2]
+            extra[s, e, 1:2] = news[1 - e, 3, pl.ds(r, 1), :] * meet
+            extra[s, e, 2:3] = decay
+
+    def conclude(s, finals):
+        kept_h = [final.astype(bf16) for final in finals]
+        sums = [dot(asks[s, e], kept_h[e]) for e in range(2)]
+        keep = tail_out.shape[2] - PAD
+        for e in range(2):
+            for j in range(sn):
+                tail_out[s, e * sn + j, 0:key_rows] = kept_h[e][j * key_rows : (j + 1) * key_rows]
+        words = []
+        for e in range(2):
+            part = sums[e][0 : 2 * PAD] + sums[e][2 * PAD : 4 * PAD] + sums[e][4 * PAD :]
+            recall, retrieve, decay = part[0:1], part[PAD : PAD + 1], extra[s, e, 2:3]
+            read = decay * recall + extra[s, e, 1:2] * (extra[s, e, 0:1] - decay * retrieve)
+            norm = lax.rsqrt(jnp.mean(read * read, axis=-1, keepdims=True) + norm_floor)
+            rest, rows = read * norm * gain_ref[...], []
+            for _ in range(3):
+                rows.append(rest.astype(bf16).astype(f32))
+                rest = rest - rows[-1]
+            words.append(jnp.concatenate(rows + [jnp.zeros((PAD - 3, extent), f32)], axis=0).astype(bf16))
+        for e in range(2):
+            for j in range(sn):
+                tail_out[s, e * sn + j, keep:] = words[e]
         for j in range(sn):
-            tail_out[s, j] = kept_h[j * key_rows : (j + 1) * key_rows]
-        sums = dot(asks[s], kept_h)
-        sums = sums[0 : 2 * PAD] + sums[2 * PAD : 4 * PAD] + sums[4 * PAD :]
-        recall, retrieve = sums[0:1], sums[PAD : PAD + 1]
-        beta_new, decay_new = nb_ref[s, h], nd_ref[s, h]
-        fresh = extra[s, 0:1] - decay_new * retrieve
-        read = decay_new * recall + (beta_new * extra[s, 1:2]) * fresh
-        norm = lax.rsqrt(jnp.mean(read * read, axis=-1, keepdims=True) + norm_floor)
-        word = read * norm * gain_ref[...]
-        for j in range(sn):
-            word_out[s, j] = word
-        for j in range(sn):
+            tail_copy(s, 1, j).start()
 
             @pl.when(j == me)
             def _():
-                tail_in[s, h] = tail_out[s, j]
-                word_in[s, h] = word_out[s, j]
+                tail_in[s, own_head(s)] = tail_out[s, j]
 
             @pl.when(j != me)
             def _():
-                for copy in tail_copies(s, j):
-                    copy.start()
+                tail_copy(s, 0, j).start()
 
     def chain_first(s):
-        @pl.when((own_head(s) < heads) & (team == 0))
+        @pl.when(owner(s) & (team == 0))
         def _():
             if groups == 1:
                 prepare(s)
             box_wait(s)
-            state = jnp.zeros((extent, extent), f32)
+            state = [jnp.zeros((extent, extent), f32)] * 2
             for i in range(g):
-                half = state.astype(bf16)
-                back_out[s, i] = half
+                half = [a.astype(bf16) for a in state]
+                for e in range(2):
+                    back_out[s, e * g + i] = half[e]
+                boxes_i = [in_box.at[s, e * g + i] for e in range(2)]
                 if i == 0:
-                    state = in_box[s, i, 1].astype(f32)
+                    state = [b[1].astype(f32) for b in boxes_i]
                 else:
-                    state = state + dot(in_box[s, i, 0], half) + in_box[s, i, 1].astype(f32)
+                    state = [a + dot(b[0], h) + b[1].astype(f32) for a, b, h in zip(state, boxes_i, half)]
             if groups > 1:
-                mid_out[s] = state.astype(bf16)
+                for e in range(2):
+                    mid_out[s, e] = state[e].astype(bf16)
                 mid_copy(s).start()
             if groups == 1:
                 conclude(s, state)
@@ -453,65 +475,69 @@
         if groups == 1:
             return
 
-        @pl.when((own_head(s) < heads) & (team > 0))
+        @pl.when(owner(s) & (team > 0))
         def _():
             prepare(s)
             box_wait(s)
+            shift, drive = [None] * 2, [None] * 2
             for i in range(g):
-                step, push = in_box[s, i, 0], in_box[s, i, 1].astype(f32)
-                if i == 0:
-                    shift, drive = step.astype(f32), push
-                else:
-                    shift, drive = (
-                        shift + step.astype(f32) + dot(step, shift.astype(bf16)),
-                        drive + push + dot(step, drive.astype(bf16)),
-                    )
-                moves[s, i * extent : (i + 1) * extent] = shift.astype(bf16)
-                drives[s, i * extent : (i + 1) * extent] = drive
+                for e in range(2):
+                    step, push = in_box[s, e * g + i, 0], in_box[s, e * g + i, 1].astype(f32)
+                    if i == 0:
+                        shift[e], drive[e] = step.astype(f32), push
+                    else:
+                        shift[e], drive[e] = (
+                            shift[e] + step.astype(f32) + dot(step, shift[e].astype(bf16)),
+                            drive[e] + push + dot(step, drive[e].astype(bf16)),
+                        )
+                    moves[s, e, i * extent : (i + 1) * extent] = shift[e].astype(bf16)
+                    drives[s, e, i * extent : (i + 1) * extent] = drive[e]
 
     def relay(s):
         if groups == 1:
             return
 
-        @pl.when((own_head(s) < heads) & (team > 0))
+        @pl.when(owner(s) & (team > 0))
         def _():
             pltpu.make_async_remote_copy(
                 src_ref=mid_out.at[s], dst_ref=mid_in.at[s], send_sem=send3.at[s], recv_sem=recv3.at[s],
                 device_id={"sp": lax.rem(me + sn - g, sn)}, device_id_type=MESH,
             ).wait_recv()
-            start = mid_in[s]
-            base = start.astype(f32)
+            start = [mid_in[s, e] for e in range(2)]
+            base = [a.astype(f32) for a in start]
             top = (g - 1) * extent
-            state = base + dot(moves[s, top:], start) + drives[s, top:]
+            state = [base[e] + dot(moves[s, e, top:], start[e]) + drives[s, e, top:] for e in range(2)]
 
             @pl.when(team < groups - 1)
             def _():
-                mid_out[s] = state.astype(bf16)
+                for e in range(2):
+                    mid_out[s, e] = state[e].astype(bf16)
                 mid_copy(s).start()
 
             @pl.when(team == groups - 1)
             def _():
                 conclude(s, state)
 
-            moved = dot(moves[s, :top], start) + drives[s, :top]
-            back_out[s, 0] = start
-            for i in range(1, g):
-                back_out[s, i] = (base + moved[(i - 1) * extent : i * extent]).astype(bf16)
+            for e in range(2):
+                moved = dot(moves[s, e, :top], start[e]) + drives[s, e, :top]
+                back_out[s, e * g] = start[e]
+                for i in range(1, g):
+                    back_out[s, e * g + i] = (base[e] + moved[(i - 1) * extent : i * extent]).astype(bf16)
             give_back(s)
 
-    def arrivals(owner, ref, sem):
+    def arrivals(own, ref, sem):
         if heads > 1:
 
-            @pl.when(owner)
+            @pl.when(own)
             def _():
                 settle(ref.at[pl.ds(0, heads - 1)], sem)
 
-        @pl.when(jnp.logical_not(owner))
+        @pl.when(jnp.logical_not(own))
         def _():
             settle(ref, sem)
 
     def finish(s):
-        arrivals(own_head(s) < heads, back_in.at[s], recv2.at[s])
+        arrivals(owner(s), back_in.at[s], recv2.at[s])
         outs = [local_out[s, h] + dot(reach[s, h], back_in[s, h]) for h in range(heads)]
         for h in range(heads):
             o = outs[h]
@@ -519,12 +545,12 @@
             mixed_ref[s * span : (s + 1) * span, h * extent : (h + 1) * extent] = (o * norm * gated[s, h]).astype(bf16)
 
     def take_tail(s):
-        source = (team == groups - 1) & (own_head(s) < heads)
-        arrivals(source, tail_in.at[s], recv4.at[s])
-        arrivals(source, word_in.at[s], recv5.at[s])
+        arrivals((team == groups - 1) & owner(s), tail_in.at[s], recv4.at[s])
+        keep = tail_in.shape[2] - PAD
         for h in range(heads):
-            cache_ref[s * heads + h] = tail_in[s, h]
-            first_ref[s : s + 1, h * extent : (h + 1) * extent] = word_in[s, h]
+            cache_ref[s * heads + h] = tail_in[s, h, 0:key_rows]
+            rows = tail_in[s, h, keep:].astype(f32)
+            first_ref[s : s + 1, h * extent : (h + 1) * extent] = rows[0:1] + rows[1:2] + rows[2:3]
 
     for s in range(seqs):
         use_whole(0, s)
@@ -534,6 +560,10 @@
             device_id={"tp": partner}, device_id_type=MESH,
         ).wait_recv()
         use_whole(1, s)
+
+    @pl.when(c == 1)
+    def _():
+        news_copy().wait_recv()
 
     for s in range(seqs):
         for ck in range(chunks):
@@ -563,12 +593,11 @@
         settle(xs.at[tme], cross_sem.at[d - 1])
         settle(xs.at[tme], fwd_sem.at[d - 1])
     for s in range(seqs):
-        own = own_head(s) < heads
-        arrivals(own, out_box.at[s], send1.at[s])
-
-        @pl.when(own)
+        arrivals(owner(s), out_box.at[s], send1.at[s])
+
+        @pl.when(owner(s))
         def _():
-            settle(back_out.at[s, pl.ds(0, g - 1)], send2.at[s])
+            settle(back_out.at[s, pl.ds(0, 2 * g - 1)], send2.at[s])
 
             @pl.when(team < groups - 1)
             def _():
@@ -576,8 +605,11 @@
 
             @pl.when(team == groups - 1)
             def _():
-                settle(tail_out.at[s, pl.ds(0, sn - 1)], send4.at[s])
-                settle(word_out.at[s, pl.ds(0, sn - 1)], send5.at[s])
+                settle(tail_out.at[s, pl.ds(0, 2 * sn - 1)], send4.at[s])
+
+    @pl.when(c == 0)
+    def _():
+        news_copy().wait_send()
 
     for s in range(seqs):
         take_tail(s)
@@ -591,6 +623,7 @@
     extent = width // heads
     pairs, key_rows = seqs * heads, extent // sn
     g = group_of(sn, heads)
+    tail = -(-key_rows // PAD) * PAD + PAD
     operands = (tokens, *weights, bw, dw, bias, rate, gain, nq, nk, nv, nb, nd)
     vmem = pl.BlockSpec(memory_space=pltpu.VMEM)
     hbm = pl.BlockSpec(memory_space=pltpu.HBM)
@@ -629,27 +662,25 @@
             pltpu.VMEM((seqs, heads, span, extent), bf16),
             pltpu.VMEM((seqs, heads, span, extent), f32),
             pltpu.VMEM((seqs, heads, 2, extent, extent), bf16),
-            pltpu.VMEM((seqs, g, 2, extent, extent), bf16),
-            pltpu.VMEM((seqs, extent, extent), bf16),
-            pltpu.VMEM((seqs, extent, extent), bf16),
-            pltpu.VMEM((seqs, g, extent, extent), bf16),
+            pltpu.VMEM((seqs, 2 * g, 2, extent, extent), bf16),
+            pltpu.VMEM((seqs, 2, extent, extent), bf16),
+            pltpu.VMEM((seqs, 2, extent, extent), bf16),
+            pltpu.VMEM((seqs, 2 * g, extent, extent), bf16),
             pltpu.VMEM((seqs, heads, extent, extent), bf16),
-            pltpu.VMEM((seqs, sn, key_rows, extent), bf16),
-            pltpu.VMEM((seqs, heads, key_rows, extent), bf16),
-            pltpu.VMEM((seqs, sn, 1, extent), f32),
-            pltpu.VMEM((seqs, heads, 1, extent), f32),
-            pltpu.VMEM((seqs, g * extent, extent), bf16),
-            pltpu.VMEM((seqs, g * extent, extent), f32),
-            pltpu.VMEM((seqs, 6 * PAD, extent), bf16),
-            pltpu.VMEM((seqs, PAD, extent), f32),
+            pltpu.VMEM((seqs, 2 * sn, tail, extent), bf16),
+            pltpu.VMEM((seqs, heads, tail, extent), bf16),
+            pltpu.VMEM((seqs, 2, g * extent, extent), bf16),
+            pltpu.VMEM((seqs, 2, g * extent, extent), f32),
+            pltpu.VMEM((seqs, 2, 6 * PAD, extent), bf16),
+            pltpu.VMEM((seqs, 2, PAD, extent), f32),
+            pltpu.VMEM((2, 5, pairs, extent), f32),
+            dma((2,)),
             dma((seqs,)),
             dma((tn,)),
             dma((chips - 1,)),
             dma((1,)),
             dma((chips - 1,)),
             dma((chips - 1, 2, seqs, chunks)),
-            dma((seqs,)),
-            dma((seqs,)),
             dma((seqs,)),
             dma((seqs,)),
             dma((seqs,)),

time: 41.8 us -> 41.9 us (level)
  no operation moved by 1% of the time
where the time goes in v5:
time: 41.9 us; the launch traced here: 41.8 us
  Pallas kernels  40.9 us (98%)
  between operations  0.81 us (2%)
    pallas_call x1, Pallas kernels, fused(): pl.pallas_call(functools.partial(fused_kernel, tn, sn, seqs, heads), out_...  40.2 us

profile of v5, /device:TPU:0, one launch (start us, length us, event | category | flops | bytes accessed | tf_op | source)
XLA Modules:
  0.0 41.8 jit_solution(5934133621241781457)
XLA Ops:
  0.6 40.2 %shard_map.166 = (bf16[384,512]{1,0:T(8,128)(2,1)S(1)}, bf16[8,16,128]{2,1,0:T(8,128)(2,1)S(1)}, f32[2,512]{1,0:T(2,128)S(1)}) custom-call(bf16[384,1024]{1,0:T(8,128)(2,1)} %bitcast.8, bf16[4096,512]{1,0:T(8,128)(2,1)} %wq_ref.1, bf16[4096,512]{1,0:T(8,128)(2,1)} %wk_ref.1, bf16[4096,512]{1,0:T(8,128)(2,1)} %wv_ref.1, bf16[4096,512]{1,0:T(8,128)(2,1)} %wg_ref.1, ...), custom_call_target="tpu_custom_call" | custom-call | tf_op jit(solution)/shard_map/pallas_call | solution.py:631
  40.8 0.8 %shard_map.167 = (bf16[2,192,512]{2,1,0:T(8,128)(2,1)}, bf16[2,4,16,128]{3,2,1,0:T(8,128)(2,1)}, f32[2,512]{1,0:T(2,128)}) custom-call(bf16[2,192,512]{2,1,0:T(8,128)(2,1)S(1)} %bitcast.6, bf16[2,4,16,128]{3,2,1,0:T(8,128)(2,1)S(1)} %bitcast.7, f32[2,512]{1,0:T(2,128)S(1)} %get-tuple-element.8.first_ref), custom_call_target="tpu_custom_call" | custom-call | tf_op jit(solution)/shard_map/pallas_call | solution.py:713

commit v6 on v5

--- a/solution.py
+++ b/solution.py
@@ -225,11 +225,11 @@
     def owner_of(s, h):
         return (s * heads + h) % g
 
-    def box_copy(s, h):
+    def box_copy(s, h, to):
         return pltpu.make_async_remote_copy(
             src_ref=out_box.at[s, h], dst_ref=in_box.at[s, (1 - c) * g + m],
             send_sem=send1.at[s], recv_sem=recv1.at[s],
-            device_id={"sp": team * g + owner_of(s, h), "tp": y * 2 + 1}, device_id_type=MESH,
+            device_id={"sp": team * g + to, "tp": y * 2 + 1}, device_id_type=MESH,
         )
 
     def boxes(s):
@@ -326,16 +326,20 @@
             def _():
                 pl.semaphore_wait(hello, 2 * (sn - 1 - me))
 
-        for h in hs:
-            own = (m == owner_of(s, h)) & (c == 1)
-
-            @pl.when(own)
-            def _():
-                in_box[s, m] = out_box[s, h]
-
-            @pl.when(jnp.logical_not(own))
-            def _():
-                box_copy(s, h).start()
+        for r in reversed(range(g)):
+            to = m
+            for bit in (b for b in (1 << i for i in range(g.bit_length())) if r & b):
+                to = to + bit * (1 - 2 * lax.rem(m // bit, 2))
+            h = lax.rem(to + g - (s * heads) % g, g)
+            if r == 0:
+
+                @pl.when((h < heads) & (c == 1))
+                def _():
+                    in_box[s, m] = out_box[s, h]
+
+            @pl.when((h < heads) & ((c == 0) | (r > 0)))
+            def _():
+                box_copy(s, h, to).start()
 
     def queries(s):
         cum, cum_t = cum_row[s], cum_col[s]
@@ -552,6 +556,11 @@
             rows = tail_in[s, h, keep:].astype(f32)
             first_ref[s : s + 1, h * extent : (h + 1) * extent] = rows[0:1] + rows[1:2] + rows[2:3]
 
+    def apart(step, *args):
+        @pl.when(me >= 0)
+        def _():
+            step(*args)
+
     for s in range(seqs):
         use_whole(0, s)
     for s in range(seqs):
@@ -571,7 +580,7 @@
                 if s == 0 or ck > 0:
                     forward(d, s, ck)
                 finish_chunk(d, s, ck, (1, 2) if ck == chunks - 1 else (1, 2, 0, 3))
-        boxes(s)
+        apart(boxes, s)
         if s > 0:
             chain_first(s - 1)
             compose(s - 1)

time: 41.9 us -> 40.5 us (0.967)
  Pallas kernels: 40.9 us -> 39.5 us
    pallas_call x1, Pallas kernels: 40.2 us -> 38.8 us  [fused(): pl.pallas_call(functools.partial(fused_kernel, tn, sn, seqs, heads), out_...]
where the time goes in v6:
time: 40.5 us; the launch traced here: 40.3 us
  Pallas kernels  39.5 us (98%)
  between operations  0.81 us (2%)
    pallas_call x1, Pallas kernels, fused(): pl.pallas_call(functools.partial(fused_kernel, tn, sn, seqs, heads), out_...  38.8 us

profile of v6, /device:TPU:0, one launch (start us, length us, event | category | flops | bytes accessed | tf_op | source)
XLA Modules:
  0.0 40.3 jit_solution(9738519534677088387)
XLA Ops:
  0.6 38.8 %shard_map.166 = (bf16[384,512]{1,0:T(8,128)(2,1)S(1)}, bf16[8,16,128]{2,1,0:T(8,128)(2,1)S(1)}, f32[2,512]{1,0:T(2,128)S(1)}) custom-call(bf16[384,1024]{1,0:T(8,128)(2,1)} %bitcast.8, bf16[4096,512]{1,0:T(8,128)(2,1)} %wq_ref.1, bf16[4096,512]{1,0:T(8,128)(2,1)} %wk_ref.1, bf16[4096,512]{1,0:T(8,128)(2,1)} %wv_ref.1, bf16[4096,512]{1,0:T(8,128)(2,1)} %wg_ref.1, ...), custom_call_target="tpu_custom_call" | custom-call | tf_op jit(solution)/shard_map/pallas_call | solution.py:640
  39.4 0.8 %shard_map.167 = (bf16[2,192,512]{2,1,0:T(8,128)(2,1)}, bf16[2,4,16,128]{3,2,1,0:T(8,128)(2,1)}, f32[2,512]{1,0:T(2,128)}) custom-call(bf16[2,192,512]{2,1,0:T(8,128)(2,1)S(1)} %bitcast.6, bf16[2,4,16,128]{3,2,1,0:T(8,128)(2,1)S(1)} %bitcast.7, f32[2,512]{1,0:T(2,128)S(1)} %get-tuple-element.8.first_ref), custom_call_target="tpu_custom_call" | custom-call | tf_op jit(solution)/shard_map/pallas_call | solution.py:722

commit v7 on v6

--- a/solution.py
+++ b/solution.py
@@ -228,7 +228,7 @@
     def box_copy(s, h, to):
         return pltpu.make_async_remote_copy(
             src_ref=out_box.at[s, h], dst_ref=in_box.at[s, (1 - c) * g + m],
-            send_sem=send1.at[s], recv_sem=recv1.at[s],
+            send_sem=send1.at[s], recv_sem=recv1.at[s, m],
             device_id={"sp": team * g + to, "tp": y * 2 + 1}, device_id_type=MESH,
         )
 
@@ -389,8 +389,14 @@
     def settle(ref, sem):
         pltpu.make_async_copy(ref, ref, sem).wait()
 
-    def box_wait(s):
-        settle(in_box.at[s, pl.ds(0, 2 * g - 1)], recv1.at[s])
+    def box_wait(s, i):
+        @pl.when(i == m)
+        def _():
+            settle(in_box.at[s, pl.ds(0, 1)], recv1.at[s, i])
+
+        @pl.when(i != m)
+        def _():
+            settle(in_box.at[s, pl.ds(0, 2)], recv1.at[s, i])
 
     def give_back(s):
         for i in range(g):
@@ -456,9 +462,9 @@
         def _():
             if groups == 1:
                 prepare(s)
-            box_wait(s)
             state = [jnp.zeros((extent, extent), f32)] * 2
             for i in range(g):
+                box_wait(s, i)
                 half = [a.astype(bf16) for a in state]
                 for e in range(2):
                     back_out[s, e * g + i] = half[e]
@@ -482,9 +488,9 @@
         @pl.when(owner(s) & (team > 0))
         def _():
             prepare(s)
-            box_wait(s)
             shift, drive = [None] * 2, [None] * 2
             for i in range(g):
+                box_wait(s, i)
                 for e in range(2):
                     step, push = in_box[s, e * g + i, 0], in_box[s, e * g + i, 1].astype(f32)
                     if i == 0:
@@ -692,7 +698,7 @@
             dma((chips - 1, 2, seqs, chunks)),
             dma((seqs,)),
             dma((seqs,)),
-            dma((seqs,)),
+            dma((seqs, g)),
             dma((seqs,)),
             dma((seqs,)),
             dma((seqs,)),

time: 40.5 us -> 40.5 us (level)
  no operation moved by 1% of the time
where the time goes in v7:
time: 40.5 us; the launch traced here: 40.4 us
  Pallas kernels  39.6 us (98%)
  between operations  0.81 us (2%)
    pallas_call x1, Pallas kernels, fused(): pl.pallas_call(functools.partial(fused_kernel, tn, sn, seqs, heads), out_...  38.8 us

profile of v7, /device:TPU:0, one launch (start us, length us, event | category | flops | bytes accessed | tf_op | source)
XLA Modules:
  0.0 40.4 jit_solution(13491594490123316161)
XLA Ops:
  0.6 38.8 %shard_map.166 = (bf16[384,512]{1,0:T(8,128)(2,1)S(1)}, bf16[8,16,128]{2,1,0:T(8,128)(2,1)S(1)}, f32[2,512]{1,0:T(2,128)S(1)}) custom-call(bf16[384,1024]{1,0:T(8,128)(2,1)} %bitcast.8, bf16[4096,512]{1,0:T(8,128)(2,1)} %wq_ref.1, bf16[4096,512]{1,0:T(8,128)(2,1)} %wk_ref.1, bf16[4096,512]{1,0:T(8,128)(2,1)} %wv_ref.1, bf16[4096,512]{1,0:T(8,128)(2,1)} %wg_ref.1, ...), custom_call_target="tpu_custom_call" | custom-call | tf_op jit(solution)/shard_map/pallas_call | solution.py:646
  39.5 0.8 %shard_map.167 = (bf16[2,192,512]{2,1,0:T(8,128)(2,1)}, bf16[2,4,16,128]{3,2,1,0:T(8,128)(2,1)}, f32[2,512]{1,0:T(2,128)}) custom-call(bf16[2,192,512]{2,1,0:T(8,128)(2,1)S(1)} %bitcast.6, bf16[2,4,16,128]{3,2,1,0:T(8,128)(2,1)S(1)} %bitcast.7, f32[2,512]{1,0:T(2,128)S(1)} %get-tuple-element.8.first_ref), custom_call_target="tpu_custom_call" | custom-call | tf_op jit(solution)/shard_map/pallas_call | solution.py:728
